TPU v7x, 512 devices: a whole 4x4x16 slice. The times are simulated.
512 devices in a mesh: sp: 32 (over z, core), tp: 16 (over y, x).
Axes of the slice: x: 4, y: 4, z: 16, core: 2. Of those that a mesh axis runs over, the one named last changes fastest.
Arguments:
- layer_input: bfloat16 [8192, 2048], P('sp', 'tp'), may hold values from -6 to 6
- doc_ids: int32 [8192], P('sp'), may hold values from 0 to 7, never falling along the last dimension, each value on 1 to 1536 neighbouring positions
- routes: int32 [8192, 2], P('sp'), may hold values from 0 to 31, all different within a row; in each aligned block of 256 rows (0 to 255, 256 to 511, ...) at most 22 rows name the same one
- route_weight: float32 [8192, 2], P('sp'), may hold values from 0.2 to 2
- pool_weight: bfloat16 [4, 512, 512], replicated, may hold values from -0.25 to 0.25
- pool_scale: float32 [2048], replicated, may hold values from 0.1 to 1.9
- norm1_gain: float32 [2048], replicated, may hold values from 0.3 to 3
- norm1_bias: float32 [2048], replicated, may hold values from -3 to 3
- expert_gate: bfloat16 [32, 2048, 2048], P('sp', None, 'tp'), may hold values from -0.125 to 0.125
- expert_up: bfloat16 [32, 2048, 2048], P('sp', None, 'tp'), may hold values from -0.125 to 0.125
- expert_down: bfloat16 [32, 2048, 2048], P('sp', 'tp'), may hold values from -0.125 to 0.125
- shared_gate: bfloat16 [2048, 1024], P(None, 'tp'), may hold values from -0.125 to 0.125
- shared_up: bfloat16 [2048, 1024], P(None, 'tp'), may hold values from -0.125 to 0.125
- shared_down: bfloat16 [1024, 2048], P('tp'), may hold values from -0.1875 to 0.1875
- norm2_gain: float32 [2048], P('tp'), may hold values from 0.1 to 1.9
- norm2_bias: float32 [2048], P('tp'), may hold values from -3 to 3
Outputs:
- settled: bfloat16 [8192, 2048], P('sp', 'tp')
Inputs may be any that keep to these rules, and one draw needn't show every extreme that they name: `routes`: in each aligned block of 256 rows no expert is named by more than 22 picks, a bound that some block reaches. `doc_ids`: never falling along the positions; each document spans 1 to 1536 positions.
All inputs are finite; a program needn't handle non-finite values.
Results may differ from a plain program's by a relative error of at most 0.013.
Values may be sent and summed in bfloat16 or wider, within the bound.
A program may use at most 64 MiB of HBM per device.

v0:
```python
import jax
import jax.numpy as jnp
from jax import lax
from jax.sharding import Mesh
from jax.sharding import PartitionSpec as P

TP = ("tp_0", "tp_1")


WINDOWS = (2, 4, 8, 16)
HALO_ROWS = 15
RESIDUAL_SCALE = 2.0**0.5
NORM_EPS = 1e-05


def shifted(shard, axis, by):
    size = lax.axis_size(axis)
    pairs = [(i, i + by) for i in range(size) if 0 <= i + by < size]
    return lax.ppermute(shard, axis, pairs)


def sent_to_all(shard, axis):
    copies = jnp.broadcast_to(shard, (lax.axis_size(axis), *shard.shape))
    return lax.all_to_all(copies, axis, split_axis=0, concat_axis=0, tiled=True)


def laid_out(parts, dim):
    parts = jnp.moveaxis(parts, 0, dim)
    lengths = parts.shape
    return parts.reshape(*lengths[:dim], lengths[dim] * lengths[dim + 1], *lengths[dim + 2 :])


def gather_directly(shard, axis, dim):
    parts = sent_to_all(shard, axis)
    return laid_out(parts, dim)


def gathered_by_axis(shard, axes, dim):
    out = shard
    for number in range(len(axes) - 1, -1, -1):
        out = lax.all_gather(out, axes[number], axis=dim, tiled=True)
    return out


def cut_along(shard, dim, size):
    lengths = shard.shape
    parts = shard.reshape(*lengths[:dim], size, lengths[dim] // size, *lengths[dim + 1 :])
    return jnp.moveaxis(parts, dim, 0)


def sent_and_summed(shard, axis, dim):
    size = lax.axis_size(axis)
    parts = lax.all_to_all(cut_along(shard, dim, size), axis, 0, 0, tiled=True)
    return jnp.sum(parts.astype(jnp.float32), axis=0)


def side_by_side(arrays, axis, dim, along):
    ends, at = ([], 0)
    for a in arrays[:-1]:
        at += a.shape[along]
        ends.append(at)
    both = jnp.concatenate(arrays, axis=along)
    return tuple(jnp.split(sent_and_summed(both, axis, dim), ends, axis=along))


def taken_together(shard, axis):
    everything = sent_to_all(shard, axis)
    return jnp.sum(everything, axis=0)


def in_one(arrays, axis):
    ends = [0]
    for a in arrays:
        ends.append(ends[-1] + a.size)
    total = taken_together(jnp.concatenate([a.ravel() for a in arrays]), axis)
    return tuple((total[b:e].reshape(a.shape) for a, b, e in zip(arrays, ends, ends[1:])))


def pooled_groups(extended, marks, halo_rows):
    length = extended.shape[0] - halo_rows
    group_width = extended.shape[1] // len(WINDOWS)
    own_mark = marks[halo_rows:]
    values = extended.astype(jnp.float32)
    outputs = []
    for group_index, window in enumerate(WINDOWS):
        section = values[:, group_index * group_width : (group_index + 1) * group_width]
        running = jnp.zeros((length, group_width), jnp.float32)
        members = jnp.zeros((length, 1), jnp.float32)
        for offset in range(window):
            first_row = halo_rows - offset
            inside = (marks[first_row : first_row + length] == own_mark).astype(jnp.float32)[
                :, None
            ]
            running = running + inside * section[first_row : first_row + length]
            members = members + inside
        outputs.append(running / members - section[halo_rows:])
    return jnp.concatenate(outputs, axis=1).astype(jnp.bfloat16)


def layer_norm_rows(values, gain, bias):
    row_mean = jnp.mean(values, axis=1, keepdims=True)
    row_var = jnp.mean(values * values, axis=1, keepdims=True) - row_mean * row_mean
    return (values - row_mean) * lax.rsqrt(row_var + NORM_EPS) * gain + bias


def shards(
    layer_input,
    doc_ids,
    routes,
    route_weight,
    pool_weight,
    pool_scale,
    norm1_gain,
    norm1_bias,
    expert_gate,
    expert_up,
    expert_down,
    shared_gate,
    shared_up,
    shared_down,
    norm2_gain,
    norm2_bias,
):
    tokens_here = layer_input.shape[0]
    width_here = layer_input.shape[1]
    doc_marks = (doc_ids + 1).astype(jnp.bfloat16)
    tail_rows, tail_marks = shifted(
        (layer_input[tokens_here - HALO_ROWS :], doc_marks[tokens_here - HALO_ROWS :]), "sp", 1
    )
    extended = jnp.concatenate([tail_rows, layer_input], axis=0)
    marks = jnp.concatenate([tail_marks, doc_marks]).astype(jnp.float32)
    whole = gather_directly(extended, TP, 1)
    model_width = whole.shape[1]
    mixed = pooled_groups(whole, marks, HALO_ROWS)
    groups = pool_weight.shape[0]
    group_width = pool_weight.shape[1]
    projected = jnp.einsum(
        "tgc,gcd->tgd",
        mixed.reshape(tokens_here, groups, group_width),
        pool_weight,
        preferred_element_type=jnp.float32,
    ).reshape(tokens_here, model_width)
    first = RESIDUAL_SCALE * whole[HALO_ROWS:].astype(jnp.float32) + projected * pool_scale
    normed = layer_norm_rows(first, norm1_gain, norm1_bias).astype(jnp.bfloat16)
    top = routes.shape[1]
    experts_all = lax.axis_size("sp")
    capacity = (tokens_here * top * 11 + 8 * experts_all - 1) // (8 * experts_all)
    flat_routes = routes.reshape(-1)
    one_hot = (flat_routes[:, None] == jnp.arange(experts_all, dtype=jnp.int32)[None, :]).astype(
        jnp.int32
    )
    ranks = jnp.sum((jnp.cumsum(one_hot, axis=0) - one_hot) * one_hot, axis=1)
    destination = flat_routes * capacity + ranks
    picked_rows = jnp.repeat(normed, top, axis=0)
    send_buffer = (
        jnp.zeros((experts_all * capacity, model_width), jnp.bfloat16)
        .at[destination]
        .set(picked_rows)
    )
    slot_grid = send_buffer.reshape(experts_all, capacity, model_width)
    own_columns = lax.dynamic_slice_in_dim(
        slot_grid, lax.axis_index(TP) * width_here, width_here, 2
    )
    moved = lax.all_to_all(own_columns, "sp", split_axis=0, concat_axis=0, tiled=True)
    arrived = gathered_by_axis(moved, TP, 2)
    arrived_rows = arrived.reshape(-1, model_width)
    gate_part = jnp.dot(arrived_rows, expert_gate[0], preferred_element_type=jnp.float32)
    up_part = jnp.dot(arrived_rows, expert_up[0], preferred_element_type=jnp.float32)
    expert_hidden = (jax.nn.silu(gate_part) * up_part).astype(jnp.bfloat16)
    routed_partial = jnp.dot(expert_hidden, expert_down[0], preferred_element_type=jnp.float32)
    shared_gate_part = jnp.dot(normed, shared_gate, preferred_element_type=jnp.float32)
    shared_up_part = jnp.dot(normed, shared_up, preferred_element_type=jnp.float32)
    shared_hidden = (jax.nn.silu(shared_gate_part) * shared_up_part).astype(jnp.bfloat16)
    shared_partial = jnp.dot(shared_hidden, shared_down, preferred_element_type=jnp.float32)
    routed_sum, shared_sum = side_by_side(
        (routed_partial.astype(jnp.bfloat16), shared_partial.astype(jnp.bfloat16)), TP, 1, 0
    )
    routed_here = routed_sum.astype(jnp.bfloat16).reshape(experts_all, capacity, width_here)
    returned = lax.all_to_all(routed_here, "sp", split_axis=0, concat_axis=0, tiled=True)
    returned_rows = returned.reshape(experts_all * capacity, width_here)
    picked_out = (
        returned_rows[destination].astype(jnp.float32).reshape(tokens_here, top, width_here)
    )
    routed_mix = jnp.sum(picked_out * route_weight[:, :, None], axis=1)
    own_normed = lax.dynamic_slice_in_dim(
        normed, lax.axis_index(TP) * width_here, width_here, 1
    ).astype(jnp.float32)
    second = RESIDUAL_SCALE * own_normed + routed_mix + shared_sum
    row_total, row_squares = in_one((jnp.sum(second, axis=1), jnp.sum(second * second, axis=1)), TP)
    row_mean = row_total / model_width
    row_var = row_squares / model_width - row_mean * row_mean
    scaled = (second - row_mean[:, None]) * lax.rsqrt(row_var + NORM_EPS)[:, None]
    return (scaled * norm2_gain + norm2_bias).astype(jnp.bfloat16)


def solution(mesh):
    split = Mesh(mesh.devices.reshape(mesh.shape["sp"], 4, 4), ("sp", "tp_0", "tp_1"))
    placed = (
        P("sp", TP),
        P("sp"),
        P("sp", None),
        P("sp", None),
        P(),
        P(),
        P(),
        P(),
        P("sp", None, TP),
        P("sp", None, TP),
        P("sp", TP, None),
        P(None, TP),
        P(None, TP),
        P(TP, None),
        P(TP),
        P(TP),
    )
    return jax.shard_map(
        shards, mesh=split, in_specs=placed, out_specs=P("sp", TP), check_vma=False
    )
```

profile of v0, /device:TPU:1, one launch (start us, length us, event | category | flops | bytes accessed | tf_op | source)
XLA Modules:
  0.0 295.8 jit_solution(17473721364915043860)
XLA Ops:
  7.4 4.9 %collective-permute-start.1 = (bf16[15]{0:T(256)(128)(2,1)S(1)}, bf16[15]{0:T(256)(128)(2,1)S(1)}, u32[]{:S(2)}, u32[]{:S(2)}) collective-permute-start(bf16[15]{0:T(256)(128)(2,1)S(1)} %slice.215), channel_id=1, source_target_pairs={{0,16},{16,32},{32,48},{48,64},{64,80},{80,96},{96,112},{112,128},... | collective-permute-start | bytes 98 | tf_op jit(solution)/shard_map/ppermute | solution.py:19
  13.1 2.0 collective-permute-start
  16.1 1.2 reduce-window.6
  19.2 1.2 broadcast_in_dim.8
  20.4 6.2 %all-to-all-start = ((bf16[16,271,128]{2,1,0:T(8,128)(2,1)}), bf16[16,271,128]{2,1,0:T(8,128)(2,1)}, u32[]{:S(2)}, u32[]{:S(2)}) async-start(bf16[16,271,128]{2,1,0:T(8,128)(2,1)} %broadcast_in_dim.8), calls=%async_computation | async-start | bytes 2228224 | tf_op jit(solution)/shard_map/all_to_all | solution.py:24
  27.3 16.3 %all-to-all-done = bf16[16,271,128]{2,1,0:T(8,128)(2,1)} async-done(((bf16[16,271,128]{2,1,0:T(8,128)(2,1)}), bf16[16,271,128]{2,1,0:T(8,128)(2,1)}, u32[]{:S(2)}, u32[]{:S(2)}) %all-to-all-start) | async-done | bytes 1110048 | tf_op jit(solution)/shard_map/all_to_all | solution.py:24
  43.5 1.5 copy.95
  47.4 1.4 fusion.69
  48.9 2.0 convolution_bitcast_fusion
  50.9 2.9 copy.71
  53.8 3.0 %copy.74 = f32[256,16,128]{2,1,0:T(8,128)} copy(f32[256,16,128]{0,2,1:T(8,128)} %bitcast.83) | data formatting | bytes 4194304 | tf_op jit(solution)/shard_map/reshape | solution.py:142
  56.9 2.9 copy.72
  59.8 3.1 %fusion.16 = (f32[256]{0:T(256)S(1)}, f32[256]{0:T(256)S(1)}, f32[256,16,128]{2,1,0:T(8,128)S(1)}) fusion(f32[256,16,128]{2,1,0:T(8,128)} %copy.74, f32[16,128]{1,0:T(8,128)S(1)} %bitcast.90, bf16[271,16,128]{2,1,0:T(8,128)(2,1)S(1)} %bitcast.86), kind=kLoop, calls=%fused_computation.31 | loop fusion | flops 3669504 | bytes 5253120 | tf_op jit(solution)/shard_map/reduce_sum | solution.py:101
  63.0 1.1 fusion.4
  64.1 2.6 broadcast_in_dim.10
  66.7 4.1 %reshape.187 = bf16[512,2048]{1,0:T(8,128)(2,1)} reshape(bf16[256,2,2048]{2,1,0:T(2,128)(2,1)} %broadcast_in_dim.10) | data formatting | bytes 4194304 | tf_op jit(solution)/shard_map/reshape | solution.py:154
  70.8 6.6 %scatter_custom_fusion = bf16[704,2048]{1,0:T(8,128)(2,1)} fusion(s32[512]{0:T(512)S(1)} %bitcast.91, bf16[512,2048]{1,0:T(8,128)(2,1)} %reshape.187, bf16[]{:T(256)} %constant.44.clone.1), kind=kCustom, calls=%fused_computation.17 | custom fusion | bytes 2884096 | tf_op jit(solution)/shard_map/scatter | solution.py:158
  77.4 4.4 %reshape.168 = bf16[32,22,2048]{2,1,0:T(8,128)(2,1)} reshape(bf16[704,2048]{1,0:T(8,128)(2,1)} %scatter_custom_fusion) | data formatting | bytes 5767168 | tf_op jit(solution)/shard_map/reshape | solution.py:160
  82.8 35.4 %all_to_all.26 = bf16[32,22,128]{2,1,0:T(8,128)(2,1)S(1)} all-to-all(bf16[32,22,128]{2,1,0:T(8,128)(2,1)S(1)} %constant_dynamic-slice_fusion), channel_id=1, replica_groups=mesh['sp'=32,'tp_0'=4,'tp_1'=4] {'sp'}, dimensions={0} | all-to-all | bytes 360448 | tf_op jit(solution)/shard_map/all_to_all | solution.py:164
  118.2 15.6 %all_gather.6 = bf16[32,22,512]{2,1,0:T(8,128)(2,1)} all-gather(bf16[32,22,128]{2,1,0:T(8,128)(2,1)S(1)} %all_to_all.26), channel_id=1, replica_groups=mesh['sp'=32,'tp_0'=4,'tp_1'=4] {'tp_1'}, dimensions={2}, use_global_device_ids=true | all-gather | bytes 901120 | tf_op jit(solution)/shard_map/all_gather | solution.py:41
  134.3 3.4 %convolution_convert_fusion.1 = bf16[256,2048]{1,0:T(8,128)(2,1)} fusion(bf16[64,2048]{1,0:T(8,128)(2,1)} %param.29, bf16[256,2048]{1,0:T(8,128)(2,1)S(1)} %fusion.4, bf16[2048,64]{0,1:T(8,128)(2,1)} %param.28, f32[256,64]{0,1:T(8,128)S(1)} %fusion.87), kind=kOutput, calls=%fused_computation.6 | convolution fusion | flops 134840320 | bytes 2686976 | tf_op jit(solution)/shard_map/dot_general | solution.py:174
  137.7 33.5 %all-gather.2.cloned.1.call-done = bf16[32,22,2048]{2,1,0:T(8,128)(2,1)} async-done(((bf16[32,22,512]{2,1,0:T(8,128)(2,1)}), bf16[32,22,2048]{2,1,0:T(8,128)(2,1)}) %all-gather.2.cloned.1.call-update) | async-done | bytes 2883600 | tf_op jit(solution)/shard_map/all_gather | solution.py:41
  171.2 4.5 %reshape.169 = bf16[704,2048]{1,0:T(8,128)(2,1)} reshape(bf16[32,22,2048]{2,1,0:T(8,128)(2,1)} %all-gather.2.cloned.1.call-done) | data formatting | bytes 5767168 | tf_op jit(solution)/shard_map/reshape | solution.py:166
  175.7 2.8 fusion.54
  178.5 6.7 %convolution_convert_fusion = bf16[704,2048]{1,0:T(8,128)(2,1)} fusion(bf16[704,2048]{1,0:T(8,128)(2,1)} %reshape.169, bf16[1,128,2048]{2,1,0:T(8,128)(2,1)} %param.26, bf16[1,2048,128]{2,1,0:T(8,128)(2,1)} %param.25, f32[704,128]{1,0:T(8,128)S(1)} %fusion.54), kind=kOutput, calls=%fused_computation.5 | convolution fusion | flops 740179968 | bytes 7176192 | tf_op jit(solution)/shard_map/dot_general | solution.py:170
  185.2 2.5 bitcast_bitcast_fusion
  187.7 52.4 %all_to_all.27 = bf16[16,960,128]{2,1,0:T(8,128)(2,1)S(1)} all-to-all(bf16[16,960,128]{2,1,0:T(8,128)(2,1)S(1)} %bitcast_bitcast_fusion), channel_id=1, replica_groups=mesh['sp'=32,'tp_0'=4,'tp_1'=4] {'tp_0','tp_1'}, dimensions={0} | all-to-all | bytes 7864320 | tf_op jit(solution)/shard_map/all_to_all | solution.py:53
  242.2 14.2 %all-to-all-start.3 = ((bf16[32,22,128]{2,1,0:T(8,128)(2,1)}), bf16[32,22,128]{2,1,0:T(8,128)(2,1)S(1)}, u32[]{:S(2)}, u32[]{:S(2)}) async-start(bf16[32,22,128]{2,1,0:T(8,128)(2,1)} %reshape.171), calls=%async_computation.3 | async-start | bytes 393216 | tf_op jit(solution)/shard_map/all_to_all | solution.py:179
  257.2 18.0 %all-to-all-done.3 = bf16[32,22,128]{2,1,0:T(8,128)(2,1)S(1)} async-done(((bf16[32,22,128]{2,1,0:T(8,128)(2,1)}), bf16[32,22,128]{2,1,0:T(8,128)(2,1)S(1)}, u32[]{:S(2)}, u32[]{:S(2)}) %all-to-all-start.3) | async-done | bytes 180256 | tf_op jit(solution)/shard_map/all_to_all | solution.py:179
  275.3 1.3 gather_fusion
  276.6 1.3 fusion.65
  279.0 9.0 %all_to_all.28 = f32[16,1,512]{2,1,0:T(1,128)S(1)} all-to-all(f32[16,1,512]{2,1,0:T(1,128)S(1)} %broadcast_in_dim.11), channel_id=1, replica_groups=mesh['sp'=32,'tp_0'=4,'tp_1'=4] {'tp_0','tp_1'}, dimensions={0} | all-to-all | bytes 65536 | tf_op jit(solution)/shard_map/all_to_all | solution.py:24
  (64 shorter events, 13.8 us)
Async XLA Ops:
  6.5 42.3 %copy-start = (bf16[4,512,512]{2,1,0:T(8,128)(2,1)S(1)}, bf16[4,512,512]{2,1,0:T(8,128)(2,1)}, u32[]{:S(2)}) copy-start(bf16[4,512,512]{2,1,0:T(8,128)(2,1)} %param.20) | copy-start | bytes 6291460
  7.4 19.6 %collective-permute-start.1 = (bf16[15]{0:T(256)(128)(2,1)S(1)}, bf16[15]{0:T(256)(128)(2,1)S(1)}, u32[]{:S(2)}, u32[]{:S(2)}) collective-permute-start(bf16[15]{0:T(256)(128)(2,1)S(1)} %slice.215), channel_id=1, source_target_pairs={{0,16},{16,32},{32,48},{48,64},{64,80},{80,96},{96,112},{112,128},... | collective-permute-start | bytes 98 | tf_op jit(solution)/shard_map/ppermute | solution.py:19
  13.1 13.5 %copy-start.7 = (s32[256,2]{0,1:T(2,128)S(1)}, s32[256,2]{0,1:T(2,128)}, u32[]{:S(2)}) copy-start(s32[256,2]{0,1:T(2,128)} %param.18) | copy-start | bytes 6148
  13.1 5.3 %collective-permute-start = (bf16[15,128]{1,0:T(8,128)(2,1)S(1)}, bf16[15,128]{1,0:T(8,128)(2,1)S(1)}, u32[]{:S(2)}, u32[]{:S(2)}) collective-permute-start(bf16[15,128]{1,0:T(8,128)(2,1)S(1)} %slice.213), channel_id=1, source_target_pairs={{0,16},{16,32},{32,48},{48,64},{64,80},{80,96},{96,112},{112,128},... | collective-permute-start | bytes 11528 | tf_op jit(solution)/shard_map/ppermute | solution.py:19
  20.4 23.2 %all-to-all-start = ((bf16[16,271,128]{2,1,0:T(8,128)(2,1)}), bf16[16,271,128]{2,1,0:T(8,128)(2,1)}, u32[]{:S(2)}, u32[]{:S(2)}) async-start(bf16[16,271,128]{2,1,0:T(8,128)(2,1)} %broadcast_in_dim.8), calls=%async_computation | async-start | bytes 2228224 | tf_op jit(solution)/shard_map/all_to_all | solution.py:24
  26.5 144.6 %all-gather.2.cloned.1.call-start = ((), (), s32[]{:S(2)}) async-start(), calls=%async_computation.5 | async-start | bytes 3932160 | tf_op jit(solution)/shard_map/all_gather | solution.py:41
  56.9 2.9 copy-start.4
  59.8 3.2 %copy-start.1 = (f32[256,2048]{1,0:T(8,128)S(1)}, f32[256,2048]{1,0:T(8,128)}, u32[]{:S(2)}) copy-start(f32[256,2048]{1,0:T(8,128)} %copy.72) | copy-start | bytes 6291460
  59.8 3.2 %copy-start.5 = (f32[2048]{0:T(1024)S(1)}, f32[2048]{0:T(1024)}, u32[]{:S(2)}) copy-start(f32[2048]{0:T(1024)} %param.23) | copy-start | bytes 24580
  59.8 3.2 %copy-start.6 = (f32[2048]{0:T(1024)S(1)}, f32[2048]{0:T(1024)}, u32[]{:S(2)}) copy-start(f32[2048]{0:T(1024)} %param.22) | copy-start | bytes 24580
  81.8 52.0 %copy-start.3 = (bf16[2048,64]{0,1:T(8,128)(2,1)S(1)}, bf16[2048,64]{0,1:T(8,128)(2,1)}, u32[]{:S(2)}) copy-start(bf16[2048,64]{0,1:T(8,128)(2,1)} %param.27) | copy-start | bytes 786436
  240.1 16.3 %copy-start.8 = (f32[256,2]{0,1:T(2,128)S(1)}, f32[256,2]{0,1:T(2,128)}, u32[]{:S(2)}) copy-start(f32[256,2]{0,1:T(2,128)} %param.19) | copy-start | bytes 6148
  240.7 0.8 copy-start.2
  241.4 46.7 %copy-start.9 = (f32[128]{0:T(128)S(1)}, f32[128]{0:T(128)}, u32[]{:S(2)}) copy-start(f32[128]{0:T(128)} %param.31) | copy-start | bytes 1540
  241.4 46.7 %copy-start.10 = (f32[128]{0:T(128)S(1)}, f32[128]{0:T(128)}, u32[]{:S(2)}) copy-start(f32[128]{0:T(128)} %param.30) | copy-start | bytes 1540
  242.2 33.0 %all-to-all-start.3 = ((bf16[32,22,128]{2,1,0:T(8,128)(2,1)}), bf16[32,22,128]{2,1,0:T(8,128)(2,1)S(1)}, u32[]{:S(2)}, u32[]{:S(2)}) async-start(bf16[32,22,128]{2,1,0:T(8,128)(2,1)} %reshape.171), calls=%async_computation.3 | async-start | bytes 393216 | tf_op jit(solution)/shard_map/all_to_all | solution.py:179
Sparse Core Ops, SparseCore 0:
  134.0 37.1 all-gather.1
where the time goes:
time: 297 us; the launch traced here: 296 us
  blocking collectives  112 us (38%)
  waiting for transfers between devices  68.4 us (23%)
  local copies, waits for them, and re-layouts  42.1 us (14%)
  starting transfers between devices  27.4 us (9%)
  other arithmetic  16.4 us (6%)
  matrix products  15.4 us (5%)
  between operations  13.7 us (5%)
    all_to_all x1, blocking collectives, sent_and_summed(): parts = lax.all_to_all(cut_along(shard, dim, size), axis, 0, 0, tiled=True)  52.4 us
    all_to_all x1, blocking collectives, shards(): lax.all_to_all(own_columns, 'sp', split_axis=0, concat_axis=0, tiled=True)  35.4 us
    all_gather x1, waiting for transfers between devices, gathered_by_axis(): out = lax.all_gather(out, axes[number], axis=dim, tiled=True)  33.5 us
    all_to_all x1, waiting for transfers between devices, shards(): lax.all_to_all(routed_here, 'sp', split_axis=0, concat_axis=0, tiled=True)  18 us
    all_to_all x1, waiting for transfers between devices, sent_to_all(): return lax.all_to_all(copies, axis, split_axis=0, concat_axis=0, tiled=True)  16.3 us
    all_gather x1, blocking collectives, gathered_by_axis(): out = lax.all_gather(out, axes[number], axis=dim, tiled=True)  15.6 us
    all_to_all x1, starting transfers between devices, shards(): lax.all_to_all(routed_here, 'sp', split_axis=0, concat_axis=0, tiled=True)  14.2 us
    all_to_all x1, blocking collectives, sent_to_all(): return lax.all_to_all(copies, axis, split_axis=0, concat_axis=0, tiled=True)  9.03 us
  transfers between devices with their start and end apart: 5, of which 4 were waited for; matrix products, arithmetic and copies ran while one was open for 4% of the time, Pallas kernels for 0%

commit v1 on v0

v1 whole, which is shorter than its diff:
```python
import functools

import jax
import jax.numpy as jnp
from jax import lax
from jax.experimental import pallas as pl
from jax.experimental.pallas import tpu as pltpu
from jax.sharding import PartitionSpec as P

MESH = pl.DeviceIdType.MESH
WINDOWS = (2, 4, 8, 16)
RESIDUAL_SCALE = 2.0**0.5
NORM_EPS = 1e-05

SP = 32
TP = 16
TOK = 256
LANES = 128
D = 2048
GROUP = 512
HALO = 16
SHARED = 64
CAP = 22
SLOT = 24
PACKED = SP * SLOT
ROWS = PACKED
PADDED = PACKED + 8

F32 = jnp.float32
BF16 = jnp.bfloat16


def iota(shape, dim):
    return lax.broadcasted_iota(jnp.int32, shape, dim)


def dot(a, b):
    return jnp.dot(a, b, preferred_element_type=F32)


def dot_nt(a, b):
    return lax.dot_general(a, b, (((1,), (1,)), ((), ())), preferred_element_type=F32)


class Gather:
    def __init__(self, buf, cuts, tp, send_sem, recv_sem):
        self.buf, self.cuts, self.tp = buf, cuts, tp
        self.send_sem, self.recv_sem = send_sem, recv_sem
        self.copies = {}

    def at(self, colour, a, b):
        y, x = self.tp // 4, lax.rem(self.tp, 4)
        dx, dy = (a, b) if colour == 0 else (b, a)
        return lax.rem(y + dy + 4, 4) * 4 + lax.rem(x + dx + 4, 4)

    def rows(self, colour, part):
        r0, r1, r2 = self.cuts[2 * colour : 2 * colour + 3]
        lo, hi = {"all": (r0, r2), "lo": (r0, r1), "hi": (r1, r2)}[part]
        return pl.ds(lo, hi - lo)

    def send(self, key, colour, block, part, to):
        number = len(self.copies)
        ref = self.buf.at[block, self.rows(colour, part)]
        copy = pltpu.make_async_remote_copy(
            src_ref=ref,
            dst_ref=ref,
            send_sem=self.send_sem.at[number],
            recv_sem=self.recv_sem.at[number],
            device_id={"tp": to},
            device_id_type=MESH,
        )
        copy.start()
        self.copies[key] = copy

    def arrived(self, *key):
        self.copies[key].wait_recv()

    def first_hop(self, c, a):
        for way in (1, -1):
            self.send(("b1", c, a, way), c, self.at(c, a, 0), "all", self.at(c, 0, way))

    def second_hop(self, c, a):
        for way, part in ((1, "lo"), (-1, "hi")):
            self.arrived("b1", c, a, way)
            block = self.at(c, a, -way)
            self.send(("b2", c, a, way), c, block, part, self.at(c, 0, way))

    def start(self):
        for c in (0, 1):
            for way in (1, -1):
                self.send(("a1", c, way), c, self.tp, "all", self.at(c, way, 0))
        for c in (0, 1):
            self.first_hop(c, 0)

    def finish(self):
        for c in (0, 1):
            for way, part in ((1, "lo"), (-1, "hi")):
                self.arrived("a1", c, way)
                self.send(("a2", c, way), c, self.at(c, -way, 0), part, self.at(c, way, 0))
        for c in (0, 1):
            self.first_hop(c, -1)
            self.first_hop(c, 1)
        for c in (0, 1):
            self.second_hop(c, 0)
        for c in (0, 1):
            self.arrived("a2", c, 1)
            self.arrived("a2", c, -1)
            self.first_hop(c, 2)
        for c in (0, 1):
            self.second_hop(c, -1)
            self.second_hop(c, 1)
        for c in (0, 1):
            self.second_hop(c, 2)
        for c in (0, 1):
            for a in (0, -1, 1, 2):
                self.arrived("b2", c, a, 1)
                self.arrived("b2", c, a, -1)

    def drain(self):
        for copy in self.copies.values():
            copy.wait_send()


def layer(
    docs, routes, weights, scale, gain1, bias1, gain2, bias2,
    x_hbm, pool_hbm, gate_hbm, up_hbm, down_hbm, sgate_hbm, sup_hbm, sdown_hbm,
    out,
    x_buf, halo, halo_docs, first, normed, slots, arrived, arrivals, hidden, shared,
    back, returned, stats, pool_w, expert_w, shared_w, down_w, sdown_w,
    load_sem, barrier_sems, g1s, g1r, g2s, g2r, g3s, g3r, g4s, g4r,
    zs, zr, rs, rr, hs, hr, ws, wr, vs, vr, ts, tr, ks, kr,
):
    sp, tp = lax.axis_index("sp"), lax.axis_index("tp")

    def sp_at(d):
        return lax.rem(sp + d, SP)

    def tp_at(d):
        return lax.rem(tp + d, TP)

    loads = [
        (x_hbm, x_buf.at[tp]),
        (pool_hbm, pool_w),
        (gate_hbm.at[0], expert_w.at[:, pl.ds(0, LANES)]),
        (up_hbm.at[0], expert_w.at[:, pl.ds(LANES, LANES)]),
        (sgate_hbm, shared_w.at[pl.ds(0, SHARED)]),
        (sup_hbm, shared_w.at[pl.ds(SHARED, SHARED)]),
        (down_hbm.at[0, :, pl.ds(pl.multiple_of(tp * LANES, LANES), LANES)], down_w.at[tp]),
        (sdown_hbm.at[:, pl.ds(pl.multiple_of(tp * LANES, LANES), LANES)], sdown_w.at[tp]),
    ]
    loads = [pltpu.make_async_copy(s, d, load_sem.at[i]) for i, (s, d) in enumerate(loads)]
    for load in loads:
        load.start()

    barrier = pltpu.get_barrier_semaphore()

    @pl.loop(1, SP)
    def _(d):
        pl.semaphore_signal(barrier, 1, device_id={"sp": sp_at(d)}, device_id_type=MESH)

    @pl.loop(1, TP)
    def _(d):
        pl.semaphore_signal(barrier, 1, device_id={"tp": tp_at(d)}, device_id_type=MESH)

    loads[0].wait()
    pl.semaphore_wait(barrier, SP - 1 + TP - 1)

    def remote(src, dst, send_sem, recv_sem, **to):
        return pltpu.make_async_remote_copy(
            src_ref=src, dst_ref=dst, send_sem=send_sem, recv_sem=recv_sem,
            device_id=to, device_id_type=MESH,
        )

    tail = remote(x_buf.at[tp, pl.ds(TOK - HALO, HALO)], halo.at[tp], ks.at[0], kr.at[0], sp=sp_at(1))
    tail_docs = remote(docs.at[:, pl.ds(LANES, LANES)], halo_docs, ks.at[1], kr.at[1], sp=sp_at(1))
    tail.start()
    tail_docs.start()
    quarter = TOK // 4
    g1 = Gather(x_buf, [quarter * i for i in range(5)], tp, g1s, g1r)
    g1.start()
    tail.wait_recv()

    def halo_copy(d):
        return remote(halo.at[tp], halo.at[tp], hs.at[d], hr.at[d], tp=tp_at(d))

    @pl.loop(1, TP)
    def _(d):
        halo_copy(d).start()

    g1.finish()

    def columns(d):
        return pl.ds(pl.multiple_of(tp_at(d) * LANES, LANES), LANES)

    def down_copy(d):
        return remote(down_hbm.at[0, :, columns(d)], down_w.at[tp], ws.at[d], wr.at[d], tp=tp_at(d))

    def sdown_copy(d):
        return remote(sdown_hbm.at[:, columns(d)], sdown_w.at[tp], vs.at[d], vr.at[d], tp=tp_at(d))

    @pl.loop(1, TP)
    def _(d):
        sdown_copy(d).start()
        down_copy(d).start()

    route_rows = routes[...]
    expert = iota((SP, TOK), 0)
    names = [(route_rows[k : k + 1] == expert).astype(F32) for k in (0, 1)]
    before = (iota((TOK, TOK), 0) < iota((TOK, TOK), 1)).astype(F32).astype(BF16)
    rank = dot((names[0] + names[1]).astype(BF16), before)
    place = expert.astype(F32) * SLOT + rank
    places = [jnp.sum(n * place, axis=0, keepdims=True) for n in names]
    row = iota((PACKED, TOK), 0).astype(F32)
    spread = ((row == places[0]) | (row == places[1])).astype(F32).astype(BF16)

    marks_row = docs[...].astype(F32)
    p, q = iota((TOK, TOK), 0), iota((TOK, TOK), 1)
    marks_col = jnp.sum(jnp.where(p == q, marks_row, 0.0), axis=1, keepdims=True)
    same = (marks_row == marks_col) & (q <= p)
    tail_docs.wait_recv()
    halo_marks = halo_docs[...][:, LANES - HALO :].astype(F32)
    hp, hq = iota((HALO, HALO), 0), iota((HALO, HALO), 1) - HALO
    halo_same = (halo_marks == marks_col[:HALO]) & (sp > 0)
    for load in loads[1:]:
        load.wait()

    @pl.loop(1, TP)
    def _(d):
        halo_copy(d).wait_recv()

    total = jnp.zeros((TOK, 1), F32)
    squares = jnp.zeros((TOK, 1), F32)
    for g, window in enumerate(WINDOWS):
        band = (same & (q > p - window)).astype(F32)
        halo_band = (halo_same & (hq > hp - window)).astype(F32)
        members = jnp.sum(band, axis=1, keepdims=True)
        halo_members = members[:HALO] + jnp.sum(halo_band, axis=1, keepdims=True)
        members = jnp.concatenate([halo_members, members[HALO:]], axis=0)
        values = jnp.concatenate([x_buf[4 * g + i] for i in range(4)], axis=1)
        halo_values = jnp.concatenate([halo[4 * g + i] for i in range(4)], axis=1)
        running = dot(band.astype(BF16), values)
        halo_running = running[:HALO] + dot(halo_band.astype(BF16), halo_values)
        running = jnp.concatenate([halo_running, running[HALO:]], axis=0)
        mixed = (running / members - values.astype(F32)).astype(BF16)
        here = pl.ds(g * GROUP, GROUP)
        projected = dot(mixed, pool_w[g]) * scale[:, here]
        value = RESIDUAL_SCALE * values.astype(F32) + projected
        first[g] = value
        total += jnp.sum(value, axis=1, keepdims=True)
        squares += jnp.sum(value * value, axis=1, keepdims=True)
    mean = total / D
    spreadness = lax.rsqrt(squares / D - mean * mean + NORM_EPS)
    for g in range(4):
        here = pl.ds(g * GROUP, GROUP)
        value = ((first[g] - mean) * spreadness * gain1[:, here] + bias1[:, here]).astype(BF16)
        for i in range(4):
            normed[4 * g + i] = value[:, i * LANES : (i + 1) * LANES]

    own_slots = dot(spread, normed[tp]).astype(BF16)
    slots[pl.ds(0, PACKED)] = own_slots

    def slot_rows(s):
        return pl.ds(pl.multiple_of(s * SLOT, 8), SLOT)

    def slot_copy(d):
        return remote(slots.at[slot_rows(sp_at(d))], arrived.at[slot_rows(sp)], zs.at[d], zr.at[d], sp=sp_at(d))

    @pl.loop(1, SP)
    def _(d):
        slot_copy(d).start()

    tokens = jnp.concatenate([normed[i] for i in range(TP)], axis=1)
    both = dot_nt(tokens, shared_w[...])
    gate_part, up_part = both[:, :SHARED], both[:, SHARED:]
    units = gate_part * jax.nn.sigmoid(gate_part) * up_part
    shared[tp] = jnp.concatenate([units[: TOK // 2], units[TOK // 2 :]], axis=1).astype(BF16)
    g2 = Gather(shared, [32 * i for i in range(5)], tp, g2s, g2r)
    g2.start()
    g2.finish()

    @pl.loop(1, SP)
    def _(d):
        slot_copy(d).wait_recv()

    own = iota((PACKED, 1), 0)
    own = (own >= sp * SLOT) & (own < sp * SLOT + SLOT)
    taken = jnp.where(own, own_slots.astype(F32), arrived[pl.ds(0, PACKED)].astype(F32))
    arrivals[tp] = taken.astype(BF16)
    step = ROWS // 4
    g3 = Gather(arrivals, [step * i for i in range(5)], tp, g3s, g3r)
    g3.start()

    @pl.loop(1, TP)
    def _(d):
        sdown_copy(d).wait_recv()

    shared_units = jnp.concatenate([shared[i] for i in range(TP)], axis=1)
    nothing = jnp.zeros((SHARED, LANES), BF16)
    parts = [sdown_w[i] for i in range(TP)]
    low = jnp.concatenate([r for part in parts for r in (part, nothing)], axis=0)
    high = jnp.concatenate([r for part in parts for r in (nothing, part)], axis=0)
    shared_out = jnp.concatenate([dot(shared_units, low), dot(shared_units, high)], axis=0)
    g3.finish()

    @pl.loop(0, 4)
    def _(i):
        rows = pl.ds(pl.multiple_of(i * step, 16), step)
        u = jnp.concatenate([arrivals[j, rows] for j in range(TP)], axis=1)
        both = dot(u, expert_w[...])
        gate_part = both[:, :LANES]
        hidden[tp, rows] = (gate_part * jax.nn.sigmoid(gate_part) * both[:, LANES:]).astype(BF16)

    g4 = Gather(hidden, [step * i for i in range(5)], tp, g4s, g4r)
    g4.start()
    g4.finish()

    @pl.loop(1, TP)
    def _(d):
        down_copy(d).wait_recv()

    @pl.loop(0, 4)
    def _(i):
        rows = pl.ds(pl.multiple_of(i * step, 16), step)
        units = jnp.concatenate([hidden[j, rows] for j in range(TP)], axis=1)
        back[rows] = dot(units, down_w[...].reshape(D, LANES)).astype(BF16)

    def back_copy(d):
        return remote(back.at[slot_rows(sp_at(d))], returned.at[slot_rows(sp)], rs.at[d], rr.at[d], sp=sp_at(d))

    @pl.loop(1, SP)
    def _(d):
        back_copy(d).start()

    rows8 = jnp.concatenate(places + [weights[...], jnp.zeros((4, TOK), F32)], axis=0)
    cols = jnp.transpose(rows8)
    column = iota((TOK, PACKED), 1).astype(F32)
    picks = jnp.where(column == cols[:, 0:1], cols[:, 2:3], 0.0)
    picks += jnp.where(column == cols[:, 1:2], cols[:, 3:4], 0.0)
    picks_hi = picks.astype(BF16)
    picks_lo = (picks - picks_hi.astype(F32)).astype(BF16)
    base = RESIDUAL_SCALE * normed[tp].astype(F32) + shared_out

    @pl.loop(1, SP)
    def _(d):
        back_copy(d).wait_recv()

    got = jnp.where(own, back[pl.ds(0, PACKED)].astype(F32), returned[pl.ds(0, PACKED)].astype(F32))
    got = got.astype(BF16)
    second = base + (dot(picks_hi, got) + dot(picks_lo, got))

    lane = iota((TOK, LANES), 1)
    total = jnp.sum(second, axis=1, keepdims=True)
    squares = jnp.sum(second * second, axis=1, keepdims=True)
    both = jnp.where(lane == 0, total, jnp.where(lane == 1, squares, 0.0))
    stats[tp] = jnp.transpose(both)[:8]

    def stats_copy(d):
        return remote(stats.at[tp], stats.at[tp], ts.at[d], tr.at[d], tp=tp_at(d))

    @pl.loop(1, TP)
    def _(d):
        stats_copy(d).start()

    @pl.loop(1, TP)
    def _(d):
        stats_copy(d).wait_recv()

    sums = stats[0]
    for i in range(1, TP):
        sums += stats[i]
    sums = jnp.transpose(sums)
    mean = sums[:, 0:1] / D
    var = sums[:, 1:2] / D - mean * mean
    settled = (second - mean) * lax.rsqrt(var + NORM_EPS)
    out[...] = (settled * gain2[...] + bias2[...]).astype(BF16)

    tail.wait_send()
    tail_docs.wait_send()
    for g in (g1, g2, g3, g4):
        g.drain()

    @pl.loop(1, TP)
    def _(d):
        halo_copy(d).wait_send()
        down_copy(d).wait_send()
        sdown_copy(d).wait_send()
        stats_copy(d).wait_send()

    @pl.loop(1, SP)
    def _(d):
        slot_copy(d).wait_send()
        back_copy(d).wait_send()


def shards(
    layer_input, doc_ids, routes, route_weight, pool_weight, pool_scale, norm1_gain, norm1_bias,
    expert_gate, expert_up, expert_down, shared_gate, shared_up, shared_down, norm2_gain, norm2_bias,
):
    vmem = pl.BlockSpec(memory_space=pltpu.VMEM)
    hbm = pl.BlockSpec(memory_space=pl.ANY)
    dma = pltpu.SemaphoreType.DMA
    scratch = [
        pltpu.VMEM((TP, TOK, LANES), BF16),
        pltpu.VMEM((TP, HALO, LANES), BF16),
        pltpu.VMEM((1, LANES), jnp.int32),
        pltpu.VMEM((4, TOK, GROUP), F32),
        pltpu.VMEM((TP, TOK, LANES), BF16),
        pltpu.VMEM((PADDED, LANES), BF16),
        pltpu.VMEM((PADDED, LANES), BF16),
        pltpu.VMEM((TP, ROWS, LANES), BF16),
        pltpu.VMEM((TP, ROWS, LANES), BF16),
        pltpu.VMEM((TP, TOK // 2, LANES), BF16),
        pltpu.VMEM((PADDED, LANES), BF16),
        pltpu.VMEM((PADDED, LANES), BF16),
        pltpu.VMEM((TP, 8, TOK), F32),
        pltpu.VMEM((4, GROUP, GROUP), BF16),
        pltpu.VMEM((D, 2 * LANES), BF16),
        pltpu.VMEM((2 * SHARED, D), BF16),
        pltpu.VMEM((TP, LANES, LANES), BF16),
        pltpu.VMEM((TP, SHARED, LANES), BF16),
        dma((8,)),
        dma((2,)),
    ]
    scratch += [dma((40,))] * 8 + [dma((SP,))] * 4 + [dma((TP,))] * 8 + [dma((2,))] * 2
    return pl.pallas_call(
        layer,
        out_shape=jax.ShapeDtypeStruct((TOK, LANES), BF16),
        in_specs=[vmem] * 8 + [hbm] * 8,
        out_specs=vmem,
        scratch_shapes=scratch,
        compiler_params=pltpu.CompilerParams(
            collective_id=0, has_side_effects=True, vmem_limit_bytes=60 * 1024 * 1024
        ),
    )(
        doc_ids.reshape(1, TOK), routes.T, route_weight.T,
        pool_scale.reshape(1, D), norm1_gain.reshape(1, D), norm1_bias.reshape(1, D),
        norm2_gain.reshape(1, LANES), norm2_bias.reshape(1, LANES),
        layer_input, pool_weight, expert_gate, expert_up, expert_down,
        shared_gate.T, shared_up.T, shared_down,
    )


def solution(mesh):
    placed = (
        P("sp", "tp"), P("sp"), P("sp", None), P("sp", None), P(), P(), P(), P(),
        P("sp", None, "tp"), P("sp", None, "tp"), P("sp", "tp", None),
        P(None, "tp"), P(None, "tp"), P("tp", None), P("tp"), P("tp"),
    )
    return jax.shard_map(
        shards, mesh=mesh, in_specs=placed, out_specs=P("sp", "tp"), check_vma=False
    )
```

time: 297 us -> 113 us (0.38)
  blocking collectives: 112 us -> 0 us
  Pallas kernels: 0 us -> 111 us
  waiting for transfers between devices: 68.4 us -> 0 us
  local copies, waits for them, and re-layouts: 42.1 us -> 1.47 us
  starting transfers between devices: 27.4 us -> 0 us
  other arithmetic: 16.4 us -> 0 us
  matrix products: 15.4 us -> 0 us
  between operations: 13.7 us -> 0.01 us
    pallas_call x0 -> x1, Pallas kernels: none -> 111 us  [shards(): pl.pallas_call(layer, out_shape=jax.ShapeDtypeStruct((TOK, LANES), BF16),...]
    all_to_all x3 -> x0, blocking collectives: 96.8 us -> none  [the longest x1 52.4 us: sent_and_summed(): parts = lax.all_to_all(cut_along(shard, dim, size), axis, 0, 0, tiled=True)]
    all_to_all x2 -> x0, waiting for transfers between devices: 34.2 us -> none  [the longest x1 18 us: shards(): lax.all_to_all(routed_here, 'sp', split_axis=0, concat_axis=0, tiled=True)]
    all_gather x1 -> x0, waiting for transfers between devices: 33.5 us -> none  [gathered_by_axis(): out = lax.all_gather(out, axes[number], axis=dim, tiled=True)]
    all_to_all x2 -> x0, starting transfers between devices: 20.4 us -> none  [the longest x1 14.2 us: shards(): lax.all_to_all(routed_here, 'sp', split_axis=0, concat_axis=0, tiled=True)]
    reshape x7 -> x0, local copies, waits for them, and re-layouts: 19.8 us -> none  [the longest x2 5.98 us: shards(): projected = jnp.einsum('tgc,gcd->tgd', mixed.reshape(tokens_here, groups,...]
    all_gather x1 -> x0, blocking collectives: 15.6 us -> none  [gathered_by_axis(): out = lax.all_gather(out, axes[number], axis=dim, tiled=True)]
    dot_general x5 -> x0, matrix products: 15.4 us -> none  [the longest x1 6.71 us: shards(): jnp.dot(expert_hidden, expert_down[0], preferred_element_type=jnp.float32)]
  transfers between devices with their start and end apart: 5 -> 0, of which waited for: 4 -> 0; matrix products, arithmetic and copies ran while one was open for 4% -> 0% of each run, Pallas kernels for 0% -> 0%
where the time goes in v1:
time: 113 us; the launch traced here: 112 us
  Pallas kernels  111 us (98%)
  local copies, waits for them, and re-layouts  1.47 us (1%)
    pallas_call x1, Pallas kernels, shards(): pl.pallas_call(layer, out_shape=jax.ShapeDtypeStruct((TOK, LANES), BF16),...  111 us

profile of v1, /device:TPU:1, one launch (start us, length us, event | category | flops | bytes accessed | tf_op | source)
XLA Modules:
  0.0 112.4 jit_solution(13884005062946080868)
XLA Ops:
  0.0 110.9 %shard_map.154 = bf16[256,128]{1,0:T(8,128)(2,1)} custom-call(s32[1,256]{1,0:T(1,128)} %bitcast.17, s32[2,256]{1,0:T(2,128)} %bitcast.15, f32[2,256]{1,0:T(2,128)} %bitcast.16, f32[1,2048]{1,0:T(1,128)} %bitcast.12, f32[1,2048]{1,0:T(1,128)} %bitcast.13, f32[1,2048]{1,0:T(1,128)} %bitcast.14, f32[1,128]{1,0:T(1,128)} %bitcast.18, f32[1,128]{1,0:T(1,128)} %bitcast.19, ...), custom_call_target="tpu_custom_call" | custom-call | tf_op jit(solution)/shard_map/pallas_call | solution.py:425
  110.9 1.5 %copy.18 = bf16[256,128]{1,0:T(8,128)(2,1)} copy(bf16[256,128]{1,0:T(8,128)(2,1)} %shard_map.154) | data formatting | bytes 131072

commit v2 on v1

v2 whole, which is shorter than its diff:
```python
import functools

import jax
import jax.numpy as jnp
from jax import lax
from jax.experimental import pallas as pl
from jax.experimental.pallas import tpu as pltpu
from jax.sharding import PartitionSpec as P

MESH = pl.DeviceIdType.MESH
WINDOWS = (2, 4, 8, 16)
RESIDUAL_SCALE = 2.0**0.5
NORM_EPS = 1e-05

SP = 32
TP = 16
TOK = 256
LANES = 128
D = 2048
GROUP = 512
HALO = 16
SHARED = 64
CAP = 22
SLOT = 24
PACKED = SP * SLOT
PADDED = PACKED + 8
NEAR = 8
HALF = SP * CAP // 2
WIDE = PACKED // 2

F32 = jnp.float32
BF16 = jnp.bfloat16


def iota(shape, dim):
    return lax.broadcasted_iota(jnp.int32, shape, dim)


def dot(a, b):
    return jnp.dot(a, b, preferred_element_type=F32)


def dot_nt(a, b):
    return lax.dot_general(a, b, (((1,), (1,)), ((), ())), preferred_element_type=F32)


class Gather:
    def __init__(self, buf, cuts, tp, send_sem, recv_sem):
        self.buf, self.cuts, self.tp = buf, cuts, tp
        self.send_sem, self.recv_sem = send_sem, recv_sem

    def at(self, colour, a, b):
        y, x = self.tp // 4, lax.rem(self.tp, 4)
        dx, dy = (a, b) if colour == 0 else (b, a)
        return lax.rem(y + dy + 4, 4) * 4 + lax.rem(x + dx + 4, 4)

    def rows(self, colour, part):
        r0, r1, r2 = self.cuts[2 * colour : 2 * colour + 3]
        lo, hi = {"all": (r0, r2), "lo": (r0, r1), "hi": (r1, r2)}[part]
        return pl.ds(lo, hi - lo)

    def copy(self, ref, number, to):
        return pltpu.make_async_remote_copy(
            src_ref=ref,
            dst_ref=ref,
            send_sem=self.send_sem.at[0],
            recv_sem=self.recv_sem.at[number],
            device_id={"tp": to},
            device_id_type=MESH,
        )

    def send(self, number, colour, block, part, to):
        self.copy(self.buf.at[block, self.rows(colour, part)], number, to).start()

    def arrived(self, number, blocks):
        self.copy(self.buf.at[pl.ds(0, blocks)], number, self.at(0, 1, 0)).wait_recv()

    def first_hop(self, number, a):
        for c in (0, 1):
            for way in (1, -1):
                self.send(number, c, self.at(c, a, 0), "all", self.at(c, 0, way))

    def second_hop(self, a):
        for c in (0, 1):
            for way, part in ((1, "lo"), (-1, "hi")):
                self.send(5, c, self.at(c, a, -way), part, self.at(c, 0, way))

    def start(self):
        for c in (0, 1):
            for way in (1, -1):
                self.send(0, c, self.tp, "all", self.at(c, way, 0))
        self.first_hop(1, 0)

    def stage(self, number):
        self.arrived(number, (2, 2, 1, 4, 2, 4)[number])
        if number == 0:
            for c in (0, 1):
                for way, part in ((1, "lo"), (-1, "hi")):
                    self.send(2, c, self.at(c, -way, 0), part, self.at(c, way, 0))
            self.first_hop(3, -1)
            self.first_hop(3, 1)
        elif number == 1:
            self.second_hop(0)
        elif number == 2:
            self.first_hop(4, 2)
        elif number == 3:
            self.second_hop(-1)
            self.second_hop(1)
        elif number == 4:
            self.second_hop(2)

    def drain(self):
        self.copy(self.buf.at[pl.ds(0, 15)], 0, self.at(0, 1, 0)).wait_send()


def layer(
    docs, routes, weights, scale, gain1, bias1, gain2, bias2,
    x_hbm, pool_hbm, gate_hbm, up_hbm, down_hbm, sgate_hbm, sup_hbm, sdown_hbm,
    out,
    x_buf, halo, halo_docs, first, normed, slots, arrived,
    near_in, far_in, near_mid, far_mid, shared, back, returned, stats,
    pool_w, expert_w, shared_w, down_w, sdown_w,
    bands, spread, picks_hi, picks_lo, squeeze, widen,
    load_sem, g1s, g1r, g2s, g2r, g3s, g3r, g4s, g4r, g5s, g5r, g6s, g6r,
    z_send, z_recv, t_send, t_recv,
):
    sp, tp = lax.axis_index("sp"), lax.axis_index("tp")

    def sp_at(d):
        return lax.rem(sp + d + SP, SP)

    def tp_at(d):
        return lax.rem(tp + d, TP)

    loads = [
        (x_hbm, x_buf.at[tp]),
        (pool_hbm, pool_w),
        (gate_hbm.at[0], expert_w.at[:, pl.ds(0, LANES)]),
        (up_hbm.at[0], expert_w.at[:, pl.ds(LANES, LANES)]),
        (sgate_hbm, shared_w.at[pl.ds(0, SHARED)]),
        (sup_hbm, shared_w.at[pl.ds(SHARED, SHARED)]),
        (down_hbm.at[0, :, pl.ds(pl.multiple_of(tp * LANES, LANES), LANES)], down_w.at[tp]),
        (sdown_hbm.at[:, pl.ds(pl.multiple_of(tp * LANES, LANES), LANES)], sdown_w.at[tp]),
    ]
    loads = [pltpu.make_async_copy(s, d, load_sem.at[i]) for i, (s, d) in enumerate(loads)]
    for load in loads:
        load.start()

    barrier = pltpu.get_barrier_semaphore()

    @pl.loop(1, SP)
    def _(d):
        pl.semaphore_signal(barrier, 1, device_id={"sp": sp_at(d)}, device_id_type=MESH)

    @pl.loop(1, TP)
    def _(d):
        pl.semaphore_signal(barrier, 1, device_id={"tp": tp_at(d)}, device_id_type=MESH)

    route_rows = routes[...]
    expert = iota((SP, TOK), 0)
    names = [(route_rows[k : k + 1] == expert).astype(F32) for k in (0, 1)]
    before = (iota((TOK, TOK), 0) < iota((TOK, TOK), 1)).astype(F32).astype(BF16)
    rank = dot((names[0] + names[1]).astype(BF16), before)
    order = jnp.bitwise_and(expert - sp + (SP + NEAR), SP - 1)
    place = order.astype(F32) * SLOT + rank
    places = [jnp.sum(n * place, axis=0, keepdims=True) for n in names]
    row = iota((PACKED, TOK), 0).astype(F32)
    spread[...] = ((row == places[0]) | (row == places[1])).astype(F32).astype(BF16)
    rows8 = jnp.concatenate(places + [weights[...], jnp.zeros((4, TOK), F32)], axis=0)
    cols = jnp.transpose(rows8)
    column = iota((TOK, PACKED), 1).astype(F32)
    picks = jnp.where(column == cols[:, 0:1], cols[:, 2:3], 0.0)
    picks += jnp.where(column == cols[:, 1:2], cols[:, 3:4], 0.0)
    high = picks.astype(BF16)
    picks_hi[...] = high
    picks_lo[...] = (picks - high.astype(F32)).astype(BF16)

    tight = iota((HALF, 1), 0).astype(F32)
    tight = tight + 2.0 * jnp.floor((tight + 0.5) * (1.0 / CAP))
    squeeze[...] = (iota((HALF, WIDE), 1).astype(F32) == tight).astype(F32).astype(BF16)
    tight = iota((1, HALF), 1).astype(F32)
    tight = tight + 2.0 * jnp.floor((tight + 0.5) * (1.0 / CAP))
    widen[...] = (iota((WIDE, HALF), 0).astype(F32) == tight).astype(F32).astype(BF16)

    marks_row = docs[...].astype(F32)
    p, q = iota((TOK, TOK), 0), iota((TOK, TOK), 1)
    marks_col = jnp.sum(jnp.where(p == q, marks_row, 0.0), axis=1, keepdims=True)
    same = (marks_row == marks_col) & (q <= p)
    members = []
    for g, window in enumerate(WINDOWS):
        band = (same & (q > p - window)).astype(F32)
        bands[g] = band.astype(BF16)
        members.append(jnp.sum(band, axis=1, keepdims=True))

    loads[0].wait()
    pl.semaphore_wait(barrier, SP - 1 + TP - 1)

    def remote(src, dst, send_sem, recv_sem, **to):
        return pltpu.make_async_remote_copy(
            src_ref=src, dst_ref=dst, send_sem=send_sem, recv_sem=recv_sem,
            device_id=to, device_id_type=MESH,
        )

    def to_all(ref, number):
        def copy(d):
            return remote(ref.at[tp], ref.at[tp], t_send.at[number], t_recv.at[number], tp=tp_at(d))

        return copy

    def all_of(ref, number):
        block = ref.at[pl.ds(0, TP - 1)]
        return remote(block, block, t_send.at[number], t_recv.at[number], tp=tp_at(1))

    tail = remote(
        x_buf.at[tp, pl.ds(TOK - HALO, HALO)], halo.at[tp], t_send.at[4], t_recv.at[4], sp=sp_at(1)
    )
    tail_docs = remote(docs.at[:, pl.ds(LANES, LANES)], halo_docs, t_send.at[5], t_recv.at[5], sp=sp_at(1))
    tail.start()
    tail_docs.start()
    g1 = Gather(x_buf, [64 * i for i in range(5)], tp, g1s, g1r)
    g1.start()
    tail.wait_recv()

    @pl.loop(1, TP)
    def _(d):
        to_all(halo, 0)(d).start()

    tail_docs.wait_recv()
    halo_marks = halo_docs[...][:, LANES - HALO :].astype(F32)
    hp, hq = iota((HALO, HALO), 0), iota((HALO, HALO), 1) - HALO
    halo_same = (halo_marks == marks_col[:HALO]) & (sp > 0)
    for number in range(6):
        g1.stage(number)

    def columns(d):
        return pl.ds(pl.multiple_of(tp_at(d) * LANES, LANES), LANES)

    @pl.loop(1, TP)
    def _(d):
        source = down_hbm.at[0, :, columns(d)]
        remote(source, down_w.at[tp], t_send.at[1], t_recv.at[1], tp=tp_at(d)).start()

    for load in loads[1:]:
        load.wait()
    all_of(halo, 0).wait_recv()

    total = jnp.zeros((TOK, 1), F32)
    squares = jnp.zeros((TOK, 1), F32)
    for g, window in enumerate(WINDOWS):
        halo_band = (halo_same & (hq > hp - window)).astype(F32)
        halo_members = members[g][:HALO] + jnp.sum(halo_band, axis=1, keepdims=True)
        share = 1.0 / jnp.concatenate([halo_members, members[g][HALO:]], axis=0)
        values = jnp.concatenate([x_buf[4 * g + i] for i in range(4)], axis=1)
        halo_values = jnp.concatenate([halo[4 * g + i] for i in range(4)], axis=1)
        running = dot(bands[g], values)
        halo_running = running[:HALO] + dot(halo_band.astype(BF16), halo_values)
        running = jnp.concatenate([halo_running, running[HALO:]], axis=0)
        mixed = (running * share - values.astype(F32)).astype(BF16)
        here = pl.ds(g * GROUP, GROUP)
        projected = dot(mixed, pool_w[g]) * scale[:, here]
        value = RESIDUAL_SCALE * values.astype(F32) + projected
        first[g] = value
        total += jnp.sum(value, axis=1, keepdims=True)
        squares += jnp.sum(value * value, axis=1, keepdims=True)
    mean = total / D
    factor = lax.rsqrt(squares / D - mean * mean + NORM_EPS)
    for g in range(4):
        here = pl.ds(g * GROUP, GROUP)
        value = ((first[g] - mean) * factor * gain1[:, here] + bias1[:, here]).astype(BF16)
        for i in range(4):
            normed[4 * g + i] = value[:, i * LANES : (i + 1) * LANES]

    def block(d):
        return pl.ds(pl.multiple_of(jnp.bitwise_and(d + (SP + NEAR), SP - 1) * SLOT, 8), SLOT)

    def over_sp(source, target, number, first_d, last_d):
        def start(d):
            remote(
                source.at[block(d)], target.at[block(-d)],
                z_send.at[number], z_recv.at[number], sp=sp_at(d),
            ).start()

        pl.loop(max(first_d, 1), last_d)(start)
        if first_d < 0:
            pl.loop(first_d, 0)(start)

    def over_sp_all(ref, number, blocks):
        rows = ref.at[pl.ds(0, blocks * SLOT)]
        return remote(rows, rows, z_send.at[number], z_recv.at[number], sp=sp_at(1))

    own_slots = dot(spread[...], normed[tp]).astype(BF16)
    slots[pl.ds(0, PACKED)] = own_slots
    over_sp(slots, arrived, 0, 1 - NEAR, NEAR + 1)
    over_sp(slots, arrived, 1, NEAR + 1, SP - NEAR + 1)

    tokens = jnp.concatenate([normed[i] for i in range(TP)], axis=1)
    both = dot_nt(tokens, shared_w[...])
    gate_part, up_part = both[:, :SHARED], both[:, SHARED:]
    units = gate_part * jax.nn.sigmoid(gate_part) * up_part
    shared[tp] = jnp.concatenate([units[: TOK // 2], units[TOK // 2 :]], axis=1).astype(BF16)
    g2 = Gather(shared, [32 * i for i in range(5)], tp, g2s, g2r)
    g2.start()

    cuts = [0, 96, 176, 272, HALF]
    mine = NEAR * SLOT
    over_sp_all(arrived, 0, 15).wait_recv()
    taken = jnp.concatenate(
        [arrived[pl.ds(0, mine)], own_slots[mine : mine + SLOT], arrived[pl.ds(mine + SLOT, WIDE - mine - SLOT)]],
        axis=0,
    )
    near_in[tp] = dot(squeeze[...], taken).astype(BF16)
    g3 = Gather(near_in, cuts, tp, g3s, g3r)
    g3.start()
    for number in range(5):
        g3.stage(number)
        g2.stage(number)

    over_sp_all(arrived, 1, 16).wait_recv()
    far_in[tp] = dot(squeeze[...], arrived[pl.ds(WIDE, WIDE)]).astype(BF16)
    g4 = Gather(far_in, cuts, tp, g4s, g4r)
    g4.start()
    g3.stage(5)
    g2.stage(5)

    def run_expert(rows_in, mid):
        @pl.loop(0, 2)
        def _(i):
            rows = pl.ds(pl.multiple_of(i * (HALF // 2), 16), HALF // 2)
            u = jnp.concatenate([rows_in[j, rows] for j in range(TP)], axis=1)
            both = dot(u, expert_w[...])
            gate_part = both[:, :LANES]
            mid[tp, rows] = (gate_part * jax.nn.sigmoid(gate_part) * both[:, LANES:]).astype(BF16)

    run_expert(near_in, near_mid)
    for number in range(5):
        g4.stage(number)

    @pl.loop(1, TP)
    def _(d):
        remote(sdown_hbm.at[:, columns(d)], sdown_w.at[tp], t_send.at[2], t_recv.at[2], tp=tp_at(d)).start()

    g4.stage(5)
    run_expert(far_in, far_mid)

    def run_down(mid, begin):
        units = jnp.concatenate([mid[j] for j in range(TP)], axis=1)
        result = dot(units, down_w[...].reshape(D, LANES)).astype(BF16)
        back[pl.ds(begin, WIDE)] = dot(widen[...], result).astype(BF16)

    g5 = Gather(far_mid, cuts, tp, g5s, g5r)
    g5.start()
    for number in range(5):
        g5.stage(number)
    g6 = Gather(near_mid, cuts, tp, g6s, g6r)
    g6.start()
    g5.stage(5)
    all_of(down_w, 1).wait_recv()
    run_down(far_mid, WIDE)
    over_sp(back, returned, 2, NEAR, SP - NEAR)
    for number in range(6):
        g6.stage(number)
    run_down(near_mid, 0)
    over_sp(back, returned, 3, -NEAR, NEAR)

    all_of(sdown_w, 2).wait_recv()
    shared_units = jnp.concatenate([shared[i] for i in range(TP)], axis=1)
    nothing = jnp.zeros((SHARED, LANES), BF16)
    parts = [sdown_w[i] for i in range(TP)]
    low = jnp.concatenate([r for part in parts for r in (part, nothing)], axis=0)
    high = jnp.concatenate([r for part in parts for r in (nothing, part)], axis=0)
    shared_out = jnp.concatenate([dot(shared_units, low), dot(shared_units, high)], axis=0)
    base = RESIDUAL_SCALE * normed[tp].astype(F32) + shared_out

    over_sp_all(returned, 2, 16).wait_recv()
    over_sp_all(returned, 3, 15).wait_recv()
    got = jnp.concatenate(
        [returned[pl.ds(0, mine)], back[pl.ds(mine, SLOT)], returned[pl.ds(mine + SLOT, PACKED - mine - SLOT)]],
        axis=0,
    )
    second = base + (dot(picks_hi[...], got) + dot(picks_lo[...], got))

    lane = iota((TOK, LANES), 1)
    total = jnp.sum(second, axis=1, keepdims=True)
    squares = jnp.sum(second * second, axis=1, keepdims=True)
    both = jnp.where(lane == 0, total, jnp.where(lane == 1, squares, 0.0))
    stats[tp] = jnp.transpose(both)[:2]

    @pl.loop(1, TP)
    def _(d):
        to_all(stats, 3)(d).start()

    all_of(stats, 3).wait_recv()
    sums = stats[0]
    for i in range(1, TP):
        sums += stats[i]
    sums = jnp.transpose(jnp.concatenate([sums, jnp.zeros((6, TOK), F32)], axis=0))
    mean = sums[:, 0:1] / D
    var = sums[:, 1:2] / D - mean * mean
    settled = (second - mean) * lax.rsqrt(var + NORM_EPS)
    out[...] = (settled * gain2[...] + bias2[...]).astype(BF16)

    tail.wait_send()
    tail_docs.wait_send()
    for g in (g1, g2, g3, g4, g5, g6):
        g.drain()
    for number, ref in enumerate((halo, down_w, sdown_w, stats)):
        all_of(ref, number).wait_send()
    for number, ref, blocks in ((0, slots, 15), (1, slots, 16), (2, back, 16), (3, back, 15)):
        over_sp_all(ref, number, blocks).wait_send()


def shards(
    layer_input, doc_ids, routes, route_weight, pool_weight, pool_scale, norm1_gain, norm1_bias,
    expert_gate, expert_up, expert_down, shared_gate, shared_up, shared_down, norm2_gain, norm2_bias,
):
    vmem = pl.BlockSpec(memory_space=pltpu.VMEM)
    hbm = pl.BlockSpec(memory_space=pl.ANY)
    dma = pltpu.SemaphoreType.DMA
    scratch = [
        pltpu.VMEM((TP, TOK, LANES), BF16),
        pltpu.VMEM((TP, HALO, LANES), BF16),
        pltpu.VMEM((1, LANES), jnp.int32),
        pltpu.VMEM((4, TOK, GROUP), F32),
        pltpu.VMEM((TP, TOK, LANES), BF16),
        pltpu.VMEM((PADDED, LANES), BF16),
        pltpu.VMEM((PADDED, LANES), BF16),
        pltpu.VMEM((TP, HALF, LANES), BF16),
        pltpu.VMEM((TP, HALF, LANES), BF16),
        pltpu.VMEM((TP, HALF, LANES), BF16),
        pltpu.VMEM((TP, HALF, LANES), BF16),
        pltpu.VMEM((TP, TOK // 2, LANES), BF16),
        pltpu.VMEM((PADDED, LANES), BF16),
        pltpu.VMEM((PADDED, LANES), BF16),
        pltpu.VMEM((TP, 2, TOK), F32),
        pltpu.VMEM((4, GROUP, GROUP), BF16),
        pltpu.VMEM((D, 2 * LANES), BF16),
        pltpu.VMEM((2 * SHARED, D), BF16),
        pltpu.VMEM((TP, LANES, LANES), BF16),
        pltpu.VMEM((TP, SHARED, LANES), BF16),
        pltpu.VMEM((4, TOK, TOK), BF16),
        pltpu.VMEM((PACKED, TOK), BF16),
        pltpu.VMEM((TOK, PACKED), BF16),
        pltpu.VMEM((TOK, PACKED), BF16),
        pltpu.VMEM((HALF, WIDE), BF16),
        pltpu.VMEM((WIDE, HALF), BF16),
        dma((8,)),
    ]
    scratch += [dma((1,)), dma((6,))] * 6 + [dma((4,))] * 2 + [dma((6,))] * 2
    return pl.pallas_call(
        layer,
        out_shape=jax.ShapeDtypeStruct((TOK, LANES), BF16),
        in_specs=[vmem] * 8 + [hbm] * 8,
        out_specs=vmem,
        scratch_shapes=scratch,
        compiler_params=pltpu.CompilerParams(
            collective_id=0, has_side_effects=True, vmem_limit_bytes=60 * 1024 * 1024
        ),
    )(
        doc_ids.reshape(1, TOK), routes.T, route_weight.T,
        pool_scale.reshape(1, D), norm1_gain.reshape(1, D), norm1_bias.reshape(1, D),
        norm2_gain.reshape(1, LANES), norm2_bias.reshape(1, LANES),
        layer_input, pool_weight, expert_gate, expert_up, expert_down,
        shared_gate.T, shared_up.T, shared_down,
    )


def solution(mesh):
    placed = (
        P("sp", "tp"), P("sp"), P("sp", None), P("sp", None), P(), P(), P(), P(),
        P("sp", None, "tp"), P("sp", None, "tp"), P("sp", "tp", None),
        P(None, "tp"), P(None, "tp"), P("tp", None), P("tp"), P("tp"),
    )
    return jax.shard_map(
        shards, mesh=mesh, in_specs=placed, out_specs=P("sp", "tp"), check_vma=False
    )
```

time: 113 us -> 111 us (0.982)
  no operation moved by 1% of the time
where the time goes in v2:
time: 111 us
  Pallas kernels  110 us (99%)
  local copies, waits for them, and re-layouts  1.47 us (1%)
    pallas_call x1, Pallas kernels, shards(): pl.pallas_call(layer, out_shape=jax.ShapeDtypeStruct((TOK, LANES), BF16),...  110 us

profile of v2, /device:TPU:1, one launch (start us, length us, event | category | flops | bytes accessed | tf_op | source)
XLA Modules:
  0.0 111.2 jit_solution(11008509345429520658)
XLA Ops:
  0.0 109.8 %shard_map.154 = bf16[256,128]{1,0:T(8,128)(2,1)} custom-call(s32[1,256]{1,0:T(1,128)} %bitcast.17, s32[2,256]{1,0:T(2,128)} %bitcast.15, f32[2,256]{1,0:T(2,128)} %bitcast.16, f32[1,2048]{1,0:T(1,128)} %bitcast.12, f32[1,2048]{1,0:T(1,128)} %bitcast.13, f32[1,2048]{1,0:T(1,128)} %bitcast.14, f32[1,128]{1,0:T(1,128)} %bitcast.18, f32[1,128]{1,0:T(1,128)} %bitcast.19, ...), custom_call_target="tpu_custom_call" | custom-call | tf_op jit(solution)/shard_map/pallas_call | solution.py:449
  109.8 1.5 %copy.18 = bf16[256,128]{1,0:T(8,128)(2,1)} copy(bf16[256,128]{1,0:T(8,128)(2,1)} %shard_map.154) | data formatting | bytes 131072

commit v3 on v2

--- a/solution.py
+++ b/solution.py
@@ -24,9 +24,33 @@
 SLOT = 24
 PACKED = SP * SLOT
 PADDED = PACKED + 8
-NEAR = 8
-HALF = SP * CAP // 2
-WIDE = PACKED // 2
+BACK = 4
+CHUNKS = (
+    tuple(range(-4, 4)),
+    tuple(range(4, 8)) + tuple(range(-8, -4)),
+    tuple(range(8, 12)) + tuple(range(-12, -8)),
+    tuple(range(12, 20)),
+)
+HALF = SP * CAP // 4
+WIDE = PACKED // 4
+CUTS = ((0, 48, 96, 144, HALF), (0, 48, 80, 128, HALF))
+ORDER = (
+    "z0 g00 g01 i00",
+    "z1 i01 g02 g03",
+    "i02 i03 i10 i11",
+    "g04 i04 i12 z2",
+    "i13 g05 i05 i14",
+    "z3 i20 i21 h00",
+    "h01 i15 i30 i31",
+    "i22 i23 h02 h03",
+    "i32 i33 h10 h11",
+    "i24 h04 h12 h13",
+    "i34 i25 h05 h14",
+    "h20 h21 i35 h15",
+    "h22 h23 h30 h31",
+    "h24 h32 h33 s0",
+    "h34 h25 h35",
+)
 
 F32 = jnp.float32
 BF16 = jnp.bfloat16
@@ -118,11 +142,10 @@
     x_hbm, pool_hbm, gate_hbm, up_hbm, down_hbm, sgate_hbm, sup_hbm, sdown_hbm,
     out,
     x_buf, halo, halo_docs, first, normed, slots, arrived,
-    near_in, far_in, near_mid, far_mid, shared, back, returned, stats,
+    in0, in1, in2, in3, mid0, mid1, mid2, mid3, shared, back, returned, stats,
     pool_w, expert_w, shared_w, down_w, sdown_w,
     bands, spread, picks_hi, picks_lo, squeeze, widen,
-    load_sem, g1s, g1r, g2s, g2r, g3s, g3r, g4s, g4r, g5s, g5r, g6s, g6r,
-    z_send, z_recv, t_send, t_recv,
+    load_sem, g_send, g_recv, z_send, z_recv, t_send, t_recv,
 ):
     sp, tp = lax.axis_index("sp"), lax.axis_index("tp")
 
@@ -161,7 +184,7 @@
     names = [(route_rows[k : k + 1] == expert).astype(F32) for k in (0, 1)]
     before = (iota((TOK, TOK), 0) < iota((TOK, TOK), 1)).astype(F32).astype(BF16)
     rank = dot((names[0] + names[1]).astype(BF16), before)
-    order = jnp.bitwise_and(expert - sp + (SP + NEAR), SP - 1)
+    order = jnp.bitwise_and(expert - sp + (SP + BACK), SP - 1)
     place = order.astype(F32) * SLOT + rank
     places = [jnp.sum(n * place, axis=0, keepdims=True) for n in names]
     row = iota((PACKED, TOK), 0).astype(F32)
@@ -217,8 +240,19 @@
     tail_docs = remote(docs.at[:, pl.ds(LANES, LANES)], halo_docs, t_send.at[5], t_recv.at[5], sp=sp_at(1))
     tail.start()
     tail_docs.start()
-    g1 = Gather(x_buf, [64 * i for i in range(5)], tp, g1s, g1r)
+    def gather(number, buf, cuts):
+        return Gather(buf, cuts, tp, g_send.at[pl.ds(number, 1)], g_recv.at[number])
+
+    g1 = gather(0, x_buf, [64 * i for i in range(5)])
     g1.start()
+
+    def send_down(a, b):
+        to = g1.at(0, a, b)
+        source = down_hbm.at[0, :, pl.ds(pl.multiple_of(to * LANES, LANES), LANES)]
+        remote(source, down_w.at[tp], t_send.at[1], t_recv.at[1], tp=to).start()
+
+    for a, b in ((1, 0), (-1, 0), (0, 1), (0, -1), (1, 1), (-1, -1), (1, -1), (-1, 1)):
+        send_down(a, b)
     tail.wait_recv()
 
     @pl.loop(1, TP)
@@ -231,14 +265,9 @@
     halo_same = (halo_marks == marks_col[:HALO]) & (sp > 0)
     for number in range(6):
         g1.stage(number)
-
-    def columns(d):
-        return pl.ds(pl.multiple_of(tp_at(d) * LANES, LANES), LANES)
-
-    @pl.loop(1, TP)
-    def _(d):
-        source = down_hbm.at[0, :, columns(d)]
-        remote(source, down_w.at[tp], t_send.at[1], t_recv.at[1], tp=tp_at(d)).start()
+        if number == 4:
+            for a, b in ((2, 0), (0, 2), (2, 1), (1, 2), (2, -1), (-1, 2), (2, 2)):
+                send_down(a, b)
 
     for load in loads[1:]:
         load.wait()
@@ -271,96 +300,99 @@
             normed[4 * g + i] = value[:, i * LANES : (i + 1) * LANES]
 
     def block(d):
-        return pl.ds(pl.multiple_of(jnp.bitwise_and(d + (SP + NEAR), SP - 1) * SLOT, 8), SLOT)
-
-    def over_sp(source, target, number, first_d, last_d):
-        def start(d):
-            remote(
-                source.at[block(d)], target.at[block(-d)],
-                z_send.at[number], z_recv.at[number], sp=sp_at(d),
-            ).start()
-
-        pl.loop(max(first_d, 1), last_d)(start)
-        if first_d < 0:
-            pl.loop(first_d, 0)(start)
-
-    def over_sp_all(ref, number, blocks):
-        rows = ref.at[pl.ds(0, blocks * SLOT)]
+        return pl.ds((d + BACK) % SP * SLOT, SLOT)
+
+    def over_sp(source, target, number, ds):
+        for d in ds:
+            if d != 0:
+                remote(
+                    source.at[block(d)], target.at[block(-d)],
+                    z_send.at[number], z_recv.at[number], sp=sp_at(d),
+                ).start()
+
+    def over_sp_all(ref, number):
+        rows = ref.at[pl.ds(0, (7 if number % 4 == 0 else 8) * SLOT)]
         return remote(rows, rows, z_send.at[number], z_recv.at[number], sp=sp_at(1))
+
+    def runs(chunk):
+        places = [(d + BACK) % SP for d in CHUNKS[chunk]]
+        if places[-1] - places[0] == 7:
+            return [(places[0] * SLOT, (places[-1] + 1) * SLOT)]
+        return [(places[i] * SLOT, (places[i + 3] + 1) * SLOT) for i in (0, 4)]
 
     own_slots = dot(spread[...], normed[tp]).astype(BF16)
     slots[pl.ds(0, PACKED)] = own_slots
-    over_sp(slots, arrived, 0, 1 - NEAR, NEAR + 1)
-    over_sp(slots, arrived, 1, NEAR + 1, SP - NEAR + 1)
+    for chunk, ds in enumerate(CHUNKS):
+        over_sp(slots, arrived, chunk, [-d for d in ds])
 
     tokens = jnp.concatenate([normed[i] for i in range(TP)], axis=1)
     both = dot_nt(tokens, shared_w[...])
     gate_part, up_part = both[:, :SHARED], both[:, SHARED:]
     units = gate_part * jax.nn.sigmoid(gate_part) * up_part
     shared[tp] = jnp.concatenate([units[: TOK // 2], units[TOK // 2 :]], axis=1).astype(BF16)
-    g2 = Gather(shared, [32 * i for i in range(5)], tp, g2s, g2r)
-    g2.start()
-
-    cuts = [0, 96, 176, 272, HALF]
-    mine = NEAR * SLOT
-    over_sp_all(arrived, 0, 15).wait_recv()
-    taken = jnp.concatenate(
-        [arrived[pl.ds(0, mine)], own_slots[mine : mine + SLOT], arrived[pl.ds(mine + SLOT, WIDE - mine - SLOT)]],
-        axis=0,
-    )
-    near_in[tp] = dot(squeeze[...], taken).astype(BF16)
-    g3 = Gather(near_in, cuts, tp, g3s, g3r)
-    g3.start()
-    for number in range(5):
-        g3.stage(number)
-        g2.stage(number)
-
-    over_sp_all(arrived, 1, 16).wait_recv()
-    far_in[tp] = dot(squeeze[...], arrived[pl.ds(WIDE, WIDE)]).astype(BF16)
-    g4 = Gather(far_in, cuts, tp, g4s, g4r)
-    g4.start()
-    g3.stage(5)
-    g2.stage(5)
-
-    def run_expert(rows_in, mid):
-        @pl.loop(0, 2)
-        def _(i):
-            rows = pl.ds(pl.multiple_of(i * (HALF // 2), 16), HALF // 2)
-            u = jnp.concatenate([rows_in[j, rows] for j in range(TP)], axis=1)
-            both = dot(u, expert_w[...])
-            gate_part = both[:, :LANES]
-            mid[tp, rows] = (gate_part * jax.nn.sigmoid(gate_part) * both[:, LANES:]).astype(BF16)
-
-    run_expert(near_in, near_mid)
-    for number in range(5):
-        g4.stage(number)
-
-    @pl.loop(1, TP)
-    def _(d):
-        remote(sdown_hbm.at[:, columns(d)], sdown_w.at[tp], t_send.at[2], t_recv.at[2], tp=tp_at(d)).start()
-
-    g4.stage(5)
-    run_expert(far_in, far_mid)
-
-    def run_down(mid, begin):
+    gathers = {"g0": gather(1, shared, [32 * i for i in range(5)])}
+    gathers["g0"].start()
+    mine, mine_end = BACK * SLOT, (BACK + 1) * SLOT
+
+    def rows_of(buf, own_rows, first_row, end):
+        if not first_row <= mine < end:
+            return [buf[pl.ds(first_row, end - first_row)]]
+        return [
+            buf[pl.ds(first_row, mine - first_row)],
+            own_rows,
+            buf[pl.ds(mine_end, end - mine_end)],
+        ]
+
+    def begin(chunk):
+        over_sp_all(arrived, chunk).wait_recv()
+        parts = [
+            part
+            for first_row, end in runs(chunk)
+            for part in rows_of(arrived, own_slots[mine:mine_end], first_row, end)
+        ]
+        buf = (in0, in1, in2, in3)[chunk]
+        buf[tp] = dot(squeeze[...], jnp.concatenate(parts, axis=0)).astype(BF16)
+        gathers["i" + str(chunk)] = gather(2 + chunk, buf, CUTS[chunk % 2])
+        gathers["i" + str(chunk)].start()
+
+    def run_expert(chunk):
+        rows_in, mid = (in0, in1, in2, in3)[chunk], (mid0, mid1, mid2, mid3)[chunk]
+        u = jnp.concatenate([rows_in[j] for j in range(TP)], axis=1)
+        both = dot(u, expert_w[...])
+        gate_part = both[:, :LANES]
+        mid[tp] = (gate_part * jax.nn.sigmoid(gate_part) * both[:, LANES:]).astype(BF16)
+        gathers["h" + str(chunk)] = gather(6 + chunk, mid, CUTS[chunk % 2])
+        gathers["h" + str(chunk)].start()
+
+    def run_down(chunk):
+        if chunk == 0:
+            all_of(down_w, 1).wait_recv()
+        mid = (mid0, mid1, mid2, mid3)[chunk]
         units = jnp.concatenate([mid[j] for j in range(TP)], axis=1)
         result = dot(units, down_w[...].reshape(D, LANES)).astype(BF16)
-        back[pl.ds(begin, WIDE)] = dot(widen[...], result).astype(BF16)
-
-    g5 = Gather(far_mid, cuts, tp, g5s, g5r)
-    g5.start()
-    for number in range(5):
-        g5.stage(number)
-    g6 = Gather(near_mid, cuts, tp, g6s, g6r)
-    g6.start()
-    g5.stage(5)
-    all_of(down_w, 1).wait_recv()
-    run_down(far_mid, WIDE)
-    over_sp(back, returned, 2, NEAR, SP - NEAR)
-    for number in range(6):
-        g6.stage(number)
-    run_down(near_mid, 0)
-    over_sp(back, returned, 3, -NEAR, NEAR)
+        result = dot(widen[...], result).astype(BF16)
+        done = 0
+        for first_row, end in runs(chunk):
+            back[pl.ds(first_row, end - first_row)] = result[done : done + end - first_row]
+            done += end - first_row
+        over_sp(back, returned, 4 + chunk, CHUNKS[chunk])
+
+    for op in [op for line in ORDER for op in line.split()]:
+        if op[0] == "z":
+            begin(int(op[1]))
+        elif op[0] == "s":
+
+            @pl.loop(1, TP)
+            def _(d):
+                source = sdown_hbm.at[:, pl.ds(pl.multiple_of(tp_at(d) * LANES, LANES), LANES)]
+                remote(source, sdown_w.at[tp], t_send.at[2], t_recv.at[2], tp=tp_at(d)).start()
+
+        else:
+            gathers[op[:2]].stage(int(op[2]))
+            if op[0] == "i" and op[2] == "5":
+                run_expert(int(op[1]))
+            elif op[0] == "h" and op[2] == "5":
+                run_down(int(op[1]))
 
     all_of(sdown_w, 2).wait_recv()
     shared_units = jnp.concatenate([shared[i] for i in range(TP)], axis=1)
@@ -371,12 +403,9 @@
     shared_out = jnp.concatenate([dot(shared_units, low), dot(shared_units, high)], axis=0)
     base = RESIDUAL_SCALE * normed[tp].astype(F32) + shared_out
 
-    over_sp_all(returned, 2, 16).wait_recv()
-    over_sp_all(returned, 3, 15).wait_recv()
-    got = jnp.concatenate(
-        [returned[pl.ds(0, mine)], back[pl.ds(mine, SLOT)], returned[pl.ds(mine + SLOT, PACKED - mine - SLOT)]],
-        axis=0,
-    )
+    for chunk in range(4):
+        over_sp_all(returned, 4 + chunk).wait_recv()
+    got = jnp.concatenate(rows_of(returned, back[pl.ds(mine, SLOT)], 0, PACKED), axis=0)
     second = base + (dot(picks_hi[...], got) + dot(picks_lo[...], got))
 
     lane = iota((TOK, LANES), 1)
@@ -401,12 +430,12 @@
 
     tail.wait_send()
     tail_docs.wait_send()
-    for g in (g1, g2, g3, g4, g5, g6):
+    for g in (g1, *gathers.values()):
         g.drain()
     for number, ref in enumerate((halo, down_w, sdown_w, stats)):
         all_of(ref, number).wait_send()
-    for number, ref, blocks in ((0, slots, 15), (1, slots, 16), (2, back, 16), (3, back, 15)):
-        over_sp_all(ref, number, blocks).wait_send()
+    for number in range(8):
+        over_sp_all(slots if number < 4 else back, number).wait_send()
 
 
 def shards(
@@ -424,10 +453,7 @@
         pltpu.VMEM((TP, TOK, LANES), BF16),
         pltpu.VMEM((PADDED, LANES), BF16),
         pltpu.VMEM((PADDED, LANES), BF16),
-        pltpu.VMEM((TP, HALF, LANES), BF16),
-        pltpu.VMEM((TP, HALF, LANES), BF16),
-        pltpu.VMEM((TP, HALF, LANES), BF16),
-        pltpu.VMEM((TP, HALF, LANES), BF16),
+        *[pltpu.VMEM((TP, HALF, LANES), BF16)] * 8,
         pltpu.VMEM((TP, TOK // 2, LANES), BF16),
         pltpu.VMEM((PADDED, LANES), BF16),
         pltpu.VMEM((PADDED, LANES), BF16),
@@ -445,7 +471,7 @@
         pltpu.VMEM((WIDE, HALF), BF16),
         dma((8,)),
     ]
-    scratch += [dma((1,)), dma((6,))] * 6 + [dma((4,))] * 2 + [dma((6,))] * 2
+    scratch += [dma((10,)), dma((10, 6)), dma((8,)), dma((8,)), dma((6,)), dma((6,))]
     return pl.pallas_call(
         layer,
         out_shape=jax.ShapeDtypeStruct((TOK, LANES), BF16),

time: 111 us -> 106 us (0.955)
  Pallas kernels: 110 us -> 104 us
    pallas_call x1, Pallas kernels: 110 us -> 104 us  [shards(): pl.pallas_call(layer, out_shape=jax.ShapeDtypeStruct((TOK, LANES), BF16),...]
where the time goes in v3:
time: 106 us; the launch traced here: 105 us
  Pallas kernels  104 us (98%)
  local copies, waits for them, and re-layouts  1.47 us (1%)
    pallas_call x1, Pallas kernels, shards(): pl.pallas_call(layer, out_shape=jax.ShapeDtypeStruct((TOK, LANES), BF16),...  104 us

profile of v3, /device:TPU:1, one launch (start us, length us, event | category | flops | bytes accessed | tf_op | source)
XLA Modules:
  0.0 105.4 jit_solution(15362177923676221718)
XLA Ops:
  0.0 103.9 %shard_map.154 = bf16[256,128]{1,0:T(8,128)(2,1)} custom-call(s32[1,256]{1,0:T(1,128)} %bitcast.17, s32[2,256]{1,0:T(2,128)} %bitcast.15, f32[2,256]{1,0:T(2,128)} %bitcast.16, f32[1,2048]{1,0:T(1,128)} %bitcast.12, f32[1,2048]{1,0:T(1,128)} %bitcast.13, f32[1,2048]{1,0:T(1,128)} %bitcast.14, f32[1,128]{1,0:T(1,128)} %bitcast.18, f32[1,128]{1,0:T(1,128)} %bitcast.19, ...), custom_call_target="tpu_custom_call" | custom-call | tf_op jit(solution)/shard_map/pallas_call | solution.py:475
  103.9 1.5 %copy.18 = bf16[256,128]{1,0:T(8,128)(2,1)} copy(bf16[256,128]{1,0:T(8,128)(2,1)} %shard_map.154) | data formatting | bytes 131072

commit v4 on v3

--- a/solution.py
+++ b/solution.py
@@ -24,32 +24,25 @@
 SLOT = 24
 PACKED = SP * SLOT
 PADDED = PACKED + 8
-BACK = 4
-CHUNKS = (
-    tuple(range(-4, 4)),
-    tuple(range(4, 8)) + tuple(range(-8, -4)),
+BACK = 8
+UNITS = (
+    tuple(range(-8, 0)),
+    tuple(range(0, 8)),
     tuple(range(8, 12)) + tuple(range(-12, -8)),
     tuple(range(12, 20)),
 )
-HALF = SP * CAP // 4
-WIDE = PACKED // 4
-CUTS = ((0, 48, 96, 144, HALF), (0, 48, 80, 128, HALF))
+CHUNKS = ((0, 1), (2,), (3,))
+ROWS = 8 * CAP
+WIDE = 8 * SLOT
+CUTS = (ROWS, 96, 80)
 ORDER = (
-    "z0 g00 g01 i00",
-    "z1 i01 g02 g03",
-    "i02 i03 i10 i11",
-    "g04 i04 i12 z2",
-    "i13 g05 i05 i14",
-    "z3 i20 i21 h00",
-    "h01 i15 i30 i31",
-    "i22 i23 h02 h03",
-    "i32 i33 h10 h11",
-    "i24 h04 h12 h13",
-    "i34 i25 h05 h14",
-    "h20 h21 i35 h15",
-    "h22 h23 h30 h31",
-    "h24 h32 h33 s0",
-    "h34 h25 h35",
+    "g00 g01 z0 i00",
+    "z1 i01 z2 i10",
+    "i11 i20 i21 i02",
+    "i12 i22 g02 h10",
+    "h11 h20 h21 h00",
+    "h01 s0 h12",
+    "h22 h02",
 )
 
 F32 = jnp.float32
@@ -69,19 +62,15 @@
 
 
 class Gather:
-    def __init__(self, buf, cuts, tp, send_sem, recv_sem):
-        self.buf, self.cuts, self.tp = buf, cuts, tp
+    def __init__(self, buf, cut, tp, send_sem, recv_sem):
+        self.buf, self.tp = buf, tp
+        self.rows = (pl.ds(0, cut), pl.ds(cut, buf.shape[1] - cut))
         self.send_sem, self.recv_sem = send_sem, recv_sem
 
     def at(self, colour, a, b):
         y, x = self.tp // 4, lax.rem(self.tp, 4)
         dx, dy = (a, b) if colour == 0 else (b, a)
         return lax.rem(y + dy + 4, 4) * 4 + lax.rem(x + dx + 4, 4)
-
-    def rows(self, colour, part):
-        r0, r1, r2 = self.cuts[2 * colour : 2 * colour + 3]
-        lo, hi = {"all": (r0, r2), "lo": (r0, r1), "hi": (r1, r2)}[part]
-        return pl.ds(lo, hi - lo)
 
     def copy(self, ref, number, to):
         return pltpu.make_async_remote_copy(
@@ -93,56 +82,40 @@
             device_id_type=MESH,
         )
 
-    def send(self, number, colour, block, part, to):
-        self.copy(self.buf.at[block, self.rows(colour, part)], number, to).start()
-
-    def arrived(self, number, blocks):
-        self.copy(self.buf.at[pl.ds(0, blocks)], number, self.at(0, 1, 0)).wait_recv()
-
-    def first_hop(self, number, a):
-        for c in (0, 1):
-            for way in (1, -1):
-                self.send(number, c, self.at(c, a, 0), "all", self.at(c, 0, way))
-
-    def second_hop(self, a):
-        for c in (0, 1):
-            for way, part in ((1, "lo"), (-1, "hi")):
-                self.send(5, c, self.at(c, a, -way), part, self.at(c, 0, way))
+    def send(self, number, colour, block, to):
+        self.copy(self.buf.at[block, self.rows[colour]], number, to).start()
+
+    def onward(self, *sources):
+        for b in (1, -1, 2):
+            for a in sources:
+                for c in (0, 1):
+                    self.send(2, c, self.at(c, a, 0), self.at(c, 0, b))
 
     def start(self):
-        for c in (0, 1):
-            for way in (1, -1):
-                self.send(0, c, self.tp, "all", self.at(c, way, 0))
-        self.first_hop(1, 0)
+        for number, ways in ((0, (1, -1)), (1, (2,))):
+            for a in ways:
+                for c in (0, 1):
+                    self.send(number, c, self.tp, self.at(c, a, 0))
+        self.onward(0)
 
     def stage(self, number):
-        self.arrived(number, (2, 2, 1, 4, 2, 4)[number])
+        self.copy(self.buf.at[pl.ds(0, (2, 1, 12)[number])], number, self.at(0, 1, 0)).wait_recv()
         if number == 0:
-            for c in (0, 1):
-                for way, part in ((1, "lo"), (-1, "hi")):
-                    self.send(2, c, self.at(c, -way, 0), part, self.at(c, way, 0))
-            self.first_hop(3, -1)
-            self.first_hop(3, 1)
+            self.onward(-1, 1)
         elif number == 1:
-            self.second_hop(0)
-        elif number == 2:
-            self.first_hop(4, 2)
-        elif number == 3:
-            self.second_hop(-1)
-            self.second_hop(1)
-        elif number == 4:
-            self.second_hop(2)
+            self.onward(2)
 
     def drain(self):
         self.copy(self.buf.at[pl.ds(0, 15)], 0, self.at(0, 1, 0)).wait_send()
 
 
 def layer(
-    docs, routes, weights, scale, gain1, bias1, gain2, bias2,
+    docs_hbm, routes_hbm, weights_hbm, scale_hbm, gain1_hbm, bias1_hbm, gain2_hbm, bias2_hbm,
     x_hbm, pool_hbm, gate_hbm, up_hbm, down_hbm, sgate_hbm, sup_hbm, sdown_hbm,
     out,
+    docs, routes, weights, scale, gain1, bias1, gain2, bias2,
     x_buf, halo, halo_docs, first, normed, slots, arrived,
-    in0, in1, in2, in3, mid0, mid1, mid2, mid3, shared, back, returned, stats,
+    in0, in1, in2, mid0, mid1, mid2, shared, back, returned, stats,
     pool_w, expert_w, shared_w, down_w, sdown_w,
     bands, spread, picks_hi, picks_lo, squeeze, widen,
     load_sem, g_send, g_recv, z_send, z_recv, t_send, t_recv,
@@ -155,7 +128,22 @@
     def tp_at(d):
         return lax.rem(tp + d, TP)
 
+    barrier = pltpu.get_barrier_semaphore()
+
+    def greet_sp(d):
+        pl.semaphore_signal(barrier, 1, device_id={"sp": sp_at(d)}, device_id_type=MESH)
+
+    pl.loop(9, 24)(greet_sp)
+
+    @pl.loop(1, TP)
+    def _(d):
+        pl.semaphore_signal(barrier, 1, device_id={"tp": tp_at(d)}, device_id_type=MESH)
+
+    pl.loop(1, 9)(greet_sp)
+    pl.loop(24, SP)(greet_sp)
+
     loads = [
+        (docs_hbm, docs), (routes_hbm, routes), (weights_hbm, weights),
         (x_hbm, x_buf.at[tp]),
         (pool_hbm, pool_w),
         (gate_hbm.at[0], expert_w.at[:, pl.ds(0, LANES)]),
@@ -164,20 +152,14 @@
         (sup_hbm, shared_w.at[pl.ds(SHARED, SHARED)]),
         (down_hbm.at[0, :, pl.ds(pl.multiple_of(tp * LANES, LANES), LANES)], down_w.at[tp]),
         (sdown_hbm.at[:, pl.ds(pl.multiple_of(tp * LANES, LANES), LANES)], sdown_w.at[tp]),
+        (scale_hbm, scale), (gain1_hbm, gain1), (bias1_hbm, bias1), (gain2_hbm, gain2), (bias2_hbm, bias2),
     ]
     loads = [pltpu.make_async_copy(s, d, load_sem.at[i]) for i, (s, d) in enumerate(loads)]
     for load in loads:
         load.start()
 
-    barrier = pltpu.get_barrier_semaphore()
-
-    @pl.loop(1, SP)
-    def _(d):
-        pl.semaphore_signal(barrier, 1, device_id={"sp": sp_at(d)}, device_id_type=MESH)
-
-    @pl.loop(1, TP)
-    def _(d):
-        pl.semaphore_signal(barrier, 1, device_id={"tp": tp_at(d)}, device_id_type=MESH)
+    for load in loads[:3]:
+        load.wait()
 
     route_rows = routes[...]
     expert = iota((SP, TOK), 0)
@@ -198,12 +180,12 @@
     picks_hi[...] = high
     picks_lo[...] = (picks - high.astype(F32)).astype(BF16)
 
-    tight = iota((HALF, 1), 0).astype(F32)
+    tight = iota((2 * ROWS, 1), 0).astype(F32)
     tight = tight + 2.0 * jnp.floor((tight + 0.5) * (1.0 / CAP))
-    squeeze[...] = (iota((HALF, WIDE), 1).astype(F32) == tight).astype(F32).astype(BF16)
-    tight = iota((1, HALF), 1).astype(F32)
+    squeeze[...] = (iota((2 * ROWS, 2 * WIDE), 1).astype(F32) == tight).astype(F32).astype(BF16)
+    tight = iota((1, ROWS), 1).astype(F32)
     tight = tight + 2.0 * jnp.floor((tight + 0.5) * (1.0 / CAP))
-    widen[...] = (iota((WIDE, HALF), 0).astype(F32) == tight).astype(F32).astype(BF16)
+    widen[...] = (iota((WIDE, ROWS), 0).astype(F32) == tight).astype(F32).astype(BF16)
 
     marks_row = docs[...].astype(F32)
     p, q = iota((TOK, TOK), 0), iota((TOK, TOK), 1)
@@ -215,7 +197,7 @@
         bands[g] = band.astype(BF16)
         members.append(jnp.sum(band, axis=1, keepdims=True))
 
-    loads[0].wait()
+    loads[3].wait()
     pl.semaphore_wait(barrier, SP - 1 + TP - 1)
 
     def remote(src, dst, send_sem, recv_sem, **to):
@@ -240,19 +222,11 @@
     tail_docs = remote(docs.at[:, pl.ds(LANES, LANES)], halo_docs, t_send.at[5], t_recv.at[5], sp=sp_at(1))
     tail.start()
     tail_docs.start()
-    def gather(number, buf, cuts):
-        return Gather(buf, cuts, tp, g_send.at[pl.ds(number, 1)], g_recv.at[number])
-
-    g1 = gather(0, x_buf, [64 * i for i in range(5)])
+    def gather(number, buf, cut):
+        return Gather(buf, cut, tp, g_send.at[pl.ds(number, 1)], g_recv.at[number])
+
+    g1 = gather(0, x_buf, TOK // 2)
     g1.start()
-
-    def send_down(a, b):
-        to = g1.at(0, a, b)
-        source = down_hbm.at[0, :, pl.ds(pl.multiple_of(to * LANES, LANES), LANES)]
-        remote(source, down_w.at[tp], t_send.at[1], t_recv.at[1], tp=to).start()
-
-    for a, b in ((1, 0), (-1, 0), (0, 1), (0, -1), (1, 1), (-1, -1), (1, -1), (-1, 1)):
-        send_down(a, b)
     tail.wait_recv()
 
     @pl.loop(1, TP)
@@ -263,13 +237,20 @@
     halo_marks = halo_docs[...][:, LANES - HALO :].astype(F32)
     hp, hq = iota((HALO, HALO), 0), iota((HALO, HALO), 1) - HALO
     halo_same = (halo_marks == marks_col[:HALO]) & (sp > 0)
-    for number in range(6):
-        g1.stage(number)
-        if number == 4:
-            for a, b in ((2, 0), (0, 2), (2, 1), (1, 2), (2, -1), (-1, 2), (2, 2)):
-                send_down(a, b)
-
-    for load in loads[1:]:
+    g1.stage(0)
+    g1.stage(1)
+
+    def columns(d):
+        return pl.ds(pl.multiple_of(tp_at(d) * LANES, LANES), LANES)
+
+    @pl.loop(1, TP)
+    def _(d):
+        source = down_hbm.at[0, :, columns(d)]
+        remote(source, down_w.at[tp], t_send.at[1], t_recv.at[1], tp=tp_at(d)).start()
+
+    g1.stage(2)
+
+    for load in loads[4:]:
         load.wait()
     all_of(halo, 0).wait_recv()
 
@@ -310,72 +291,79 @@
                     z_send.at[number], z_recv.at[number], sp=sp_at(d),
                 ).start()
 
-    def over_sp_all(ref, number):
-        rows = ref.at[pl.ds(0, (7 if number % 4 == 0 else 8) * SLOT)]
+    def over_sp_all(ref, number, blocks):
+        rows = ref.at[pl.ds(0, blocks * SLOT)]
         return remote(rows, rows, z_send.at[number], z_recv.at[number], sp=sp_at(1))
 
-    def runs(chunk):
-        places = [(d + BACK) % SP for d in CHUNKS[chunk]]
+    def runs(unit):
+        places = [(d + BACK) % SP for d in UNITS[unit]]
         if places[-1] - places[0] == 7:
             return [(places[0] * SLOT, (places[-1] + 1) * SLOT)]
         return [(places[i] * SLOT, (places[i + 3] + 1) * SLOT) for i in (0, 4)]
 
-    own_slots = dot(spread[...], normed[tp]).astype(BF16)
-    slots[pl.ds(0, PACKED)] = own_slots
-    for chunk, ds in enumerate(CHUNKS):
-        over_sp(slots, arrived, chunk, [-d for d in ds])
+    near = 18 * SLOT
+    own_slots = dot(spread[pl.ds(0, near)], normed[tp]).astype(BF16)
+    slots[pl.ds(0, near)] = own_slots
+    over_sp(slots, arrived, 0, [-d for unit in CHUNKS[0] for d in UNITS[unit]])
+    rest = pl.ds(near, PACKED - near)
+    slots[rest] = dot(spread[rest], normed[tp]).astype(BF16)
+    for chunk in (1, 2):
+        over_sp(slots, arrived, chunk, [-d for d in UNITS[chunk + 1]])
 
     tokens = jnp.concatenate([normed[i] for i in range(TP)], axis=1)
     both = dot_nt(tokens, shared_w[...])
     gate_part, up_part = both[:, :SHARED], both[:, SHARED:]
     units = gate_part * jax.nn.sigmoid(gate_part) * up_part
     shared[tp] = jnp.concatenate([units[: TOK // 2], units[TOK // 2 :]], axis=1).astype(BF16)
-    gathers = {"g0": gather(1, shared, [32 * i for i in range(5)])}
+    gathers = {"g0": gather(1, shared, TOK // 4)}
     gathers["g0"].start()
     mine, mine_end = BACK * SLOT, (BACK + 1) * SLOT
+    ins, mids = (in0, in1, in2), (mid0, mid1, mid2)
 
     def rows_of(buf, own_rows, first_row, end):
+        parts = [(first_row, mine), (mine, mine_end), (mine_end, end)]
         if not first_row <= mine < end:
-            return [buf[pl.ds(first_row, end - first_row)]]
-        return [
-            buf[pl.ds(first_row, mine - first_row)],
-            own_rows,
-            buf[pl.ds(mine_end, end - mine_end)],
-        ]
+            parts = [(first_row, end)]
+        parts = [(lo, hi) for lo, hi in parts if lo < hi]
+        return [own_rows if lo == mine else buf[pl.ds(lo, hi - lo)] for lo, hi in parts]
 
     def begin(chunk):
-        over_sp_all(arrived, chunk).wait_recv()
+        over_sp_all(arrived, chunk, 15 if chunk == 0 else 8).wait_recv()
         parts = [
             part
-            for first_row, end in runs(chunk)
+            for unit in CHUNKS[chunk]
+            for first_row, end in runs(unit)
             for part in rows_of(arrived, own_slots[mine:mine_end], first_row, end)
         ]
-        buf = (in0, in1, in2, in3)[chunk]
-        buf[tp] = dot(squeeze[...], jnp.concatenate(parts, axis=0)).astype(BF16)
-        gathers["i" + str(chunk)] = gather(2 + chunk, buf, CUTS[chunk % 2])
+        count = len(CHUNKS[chunk])
+        tight = squeeze[pl.ds(0, count * ROWS), pl.ds(0, count * WIDE)]
+        ins[chunk][tp] = dot(tight, jnp.concatenate(parts, axis=0)).astype(BF16)
+        gathers["i" + str(chunk)] = gather(2 + chunk, ins[chunk], CUTS[chunk])
         gathers["i" + str(chunk)].start()
 
     def run_expert(chunk):
-        rows_in, mid = (in0, in1, in2, in3)[chunk], (mid0, mid1, mid2, mid3)[chunk]
-        u = jnp.concatenate([rows_in[j] for j in range(TP)], axis=1)
-        both = dot(u, expert_w[...])
-        gate_part = both[:, :LANES]
-        mid[tp] = (gate_part * jax.nn.sigmoid(gate_part) * both[:, LANES:]).astype(BF16)
-        gathers["h" + str(chunk)] = gather(6 + chunk, mid, CUTS[chunk % 2])
+        for i in range(len(CHUNKS[chunk])):
+            rows = pl.ds(i * ROWS, ROWS)
+            u = jnp.concatenate([ins[chunk][j, rows] for j in range(TP)], axis=1)
+            both = dot(u, expert_w[...])
+            gate_part = both[:, :LANES]
+            value = gate_part * jax.nn.sigmoid(gate_part) * both[:, LANES:]
+            mids[chunk][tp, rows] = value.astype(BF16)
+        gathers["h" + str(chunk)] = gather(5 + chunk, mids[chunk], CUTS[chunk])
         gathers["h" + str(chunk)].start()
 
     def run_down(chunk):
-        if chunk == 0:
+        if chunk == 1:
             all_of(down_w, 1).wait_recv()
-        mid = (mid0, mid1, mid2, mid3)[chunk]
-        units = jnp.concatenate([mid[j] for j in range(TP)], axis=1)
-        result = dot(units, down_w[...].reshape(D, LANES)).astype(BF16)
-        result = dot(widen[...], result).astype(BF16)
-        done = 0
-        for first_row, end in runs(chunk):
-            back[pl.ds(first_row, end - first_row)] = result[done : done + end - first_row]
-            done += end - first_row
-        over_sp(back, returned, 4 + chunk, CHUNKS[chunk])
+        for i, unit in enumerate(CHUNKS[chunk]):
+            units = [mids[chunk][j, pl.ds(i * ROWS, ROWS)] for j in range(TP)]
+            result = dot(jnp.concatenate(units, axis=1), down_w[...].reshape(D, LANES))
+            result = dot(widen[...], result.astype(BF16)).astype(BF16)
+            done = 0
+            for first_row, end in runs(unit):
+                back[pl.ds(first_row, end - first_row)] = result[done : done + end - first_row]
+                done += end - first_row
+            over_sp(back, returned, 3 + unit, UNITS[unit])
 
     for op in [op for line in ORDER for op in line.split()]:
         if op[0] == "z":
@@ -384,14 +372,14 @@
 
             @pl.loop(1, TP)
             def _(d):
-                source = sdown_hbm.at[:, pl.ds(pl.multiple_of(tp_at(d) * LANES, LANES), LANES)]
+                source = sdown_hbm.at[:, columns(d)]
                 remote(source, sdown_w.at[tp], t_send.at[2], t_recv.at[2], tp=tp_at(d)).start()
 
         else:
             gathers[op[:2]].stage(int(op[2]))
-            if op[0] == "i" and op[2] == "5":
+            if op[0] == "i" and op[2] == "2":
                 run_expert(int(op[1]))
-            elif op[0] == "h" and op[2] == "5":
+            elif op[0] == "h" and op[2] == "2":
                 run_down(int(op[1]))
 
     all_of(sdown_w, 2).wait_recv()
@@ -403,8 +391,8 @@
     shared_out = jnp.concatenate([dot(shared_units, low), dot(shared_units, high)], axis=0)
     base = RESIDUAL_SCALE * normed[tp].astype(F32) + shared_out
 
-    for chunk in range(4):
-        over_sp_all(returned, 4 + chunk).wait_recv()
+    for unit in (2, 3, 0, 1):
+        over_sp_all(returned, 3 + unit, 7 if unit == 1 else 8).wait_recv()
     got = jnp.concatenate(rows_of(returned, back[pl.ds(mine, SLOT)], 0, PACKED), axis=0)
     second = base + (dot(picks_hi[...], got) + dot(picks_lo[...], got))
 
@@ -434,8 +422,8 @@
         g.drain()
     for number, ref in enumerate((halo, down_w, sdown_w, stats)):
         all_of(ref, number).wait_send()
-    for number in range(8):
-        over_sp_all(slots if number < 4 else back, number).wait_send()
+    for number, blocks in enumerate((15, 8, 8, 8, 7, 8, 8)):
+        over_sp_all(slots if number < 3 else back, number, blocks).wait_send()
 
 
 def shards(
@@ -446,6 +434,11 @@
     hbm = pl.BlockSpec(memory_space=pl.ANY)
     dma = pltpu.SemaphoreType.DMA
     scratch = [
+        pltpu.VMEM((1, TOK), jnp.int32),
+        pltpu.VMEM((2, TOK), jnp.int32),
+        pltpu.VMEM((2, TOK), F32),
+        *[pltpu.VMEM((1, D), F32)] * 3,
+        *[pltpu.VMEM((1, LANES), F32)] * 2,
         pltpu.VMEM((TP, TOK, LANES), BF16),
         pltpu.VMEM((TP, HALO, LANES), BF16),
         pltpu.VMEM((1, LANES), jnp.int32),
@@ -453,7 +446,7 @@
         pltpu.VMEM((TP, TOK, LANES), BF16),
         pltpu.VMEM((PADDED, LANES), BF16),
         pltpu.VMEM((PADDED, LANES), BF16),
-        *[pltpu.VMEM((TP, HALF, LANES), BF16)] * 8,
+        *[pltpu.VMEM((TP, n * ROWS, LANES), BF16) for n in (2, 1, 1) * 2],
         pltpu.VMEM((TP, TOK // 2, LANES), BF16),
         pltpu.VMEM((PADDED, LANES), BF16),
         pltpu.VMEM((PADDED, LANES), BF16),
@@ -467,15 +460,15 @@
         pltpu.VMEM((PACKED, TOK), BF16),
         pltpu.VMEM((TOK, PACKED), BF16),
         pltpu.VMEM((TOK, PACKED), BF16),
-        pltpu.VMEM((HALF, WIDE), BF16),
-        pltpu.VMEM((WIDE, HALF), BF16),
-        dma((8,)),
+        pltpu.VMEM((2 * ROWS, 2 * WIDE), BF16),
+        pltpu.VMEM((WIDE, ROWS), BF16),
+        dma((16,)),
     ]
-    scratch += [dma((10,)), dma((10, 6)), dma((8,)), dma((8,)), dma((6,)), dma((6,))]
+    scratch += [dma((8,)), dma((8, 3)), dma((7,)), dma((7,)), dma((6,)), dma((6,))]
     return pl.pallas_call(
         layer,
         out_shape=jax.ShapeDtypeStruct((TOK, LANES), BF16),
-        in_specs=[vmem] * 8 + [hbm] * 8,
+        in_specs=[hbm] * 16,
         out_specs=vmem,
         scratch_shapes=scratch,
         compiler_params=pltpu.CompilerParams(

time: 106 us -> 98.1 us (0.925)
  Pallas kernels: 104 us -> 96.5 us
    pallas_call x1, Pallas kernels: 104 us -> 96.5 us  [shards(): pl.pallas_call(layer, out_shape=jax.ShapeDtypeStruct((TOK, LANES), BF16),...]
where the time goes in v4:
time: 98.1 us; the launch traced here: 98 us
  Pallas kernels  96.5 us (98%)
  local copies, waits for them, and re-layouts  1.47 us (1%)
    pallas_call x1, Pallas kernels, shards(): pl.pallas_call(layer, out_shape=jax.ShapeDtypeStruct((TOK, LANES), BF16),...  96.5 us

profile of v4, /device:TPU:1, one launch (start us, length us, event | category | flops | bytes accessed | tf_op | source)
XLA Modules:
  0.0 98.0 jit_solution(4100903008584091863)
XLA Ops:
  0.0 96.5 %shard_map.154 = bf16[256,128]{1,0:T(8,128)(2,1)} custom-call(s32[1,256]{1,0:T(1,128)} %bitcast.17, s32[2,256]{1,0:T(2,128)} %bitcast.15, f32[2,256]{1,0:T(2,128)} %bitcast.16, f32[1,2048]{1,0:T(1,128)} %bitcast.12, f32[1,2048]{1,0:T(1,128)} %bitcast.13, f32[1,2048]{1,0:T(1,128)} %bitcast.14, f32[1,128]{1,0:T(1,128)} %bitcast.18, f32[1,128]{1,0:T(1,128)} %bitcast.19, ...), custom_call_target="tpu_custom_call" | custom-call | tf_op jit(solution)/shard_map/pallas_call | solution.py:468
  96.5 1.5 %copy.18 = bf16[256,128]{1,0:T(8,128)(2,1)} copy(bf16[256,128]{1,0:T(8,128)(2,1)} %shard_map.154) | data formatting | bytes 131072

commit v5 on v4

--- a/solution.py
+++ b/solution.py
@@ -34,15 +34,17 @@
 CHUNKS = ((0, 1), (2,), (3,))
 ROWS = 8 * CAP
 WIDE = 8 * SLOT
-CUTS = (ROWS, 96, 80)
+CUTS = ((96, 176, 272), (48, 96, 144), (48, 80, 128))
 ORDER = (
-    "g00 g01 z0 i00",
-    "z1 i01 z2 i10",
-    "i11 i20 i21 i02",
-    "i12 i22 g02 h10",
-    "h11 h20 h21 h00",
-    "h01 s0 h12",
-    "h22 h02",
+    "g00 g02 s0 z0",
+    "z1 i00 i01 i02",
+    "i10 i11 i12 z2",
+    "i03 i13 i04 i14",
+    "i20 i21 i22 i05",
+    "i23 i24 i15 i25",
+    "h10 h12 h20 h22",
+    "g05 h00 h15 h02",
+    "h25 h05",
 )
 
 F32 = jnp.float32
@@ -62,9 +64,14 @@
 
 
 class Gather:
-    def __init__(self, buf, cut, tp, send_sem, recv_sem):
-        self.buf, self.tp = buf, tp
-        self.rows = (pl.ds(0, cut), pl.ds(cut, buf.shape[1] - cut))
+    def __init__(self, buf, cuts, tp, send_sem, recv_sem, relay=False):
+        self.buf, self.tp, self.relay = buf, tp, relay
+        c0, c1, c2 = cuts
+        end = buf.shape[1]
+        whole = (pl.ds(0, c1), pl.ds(c1, end - c1))
+        low = (pl.ds(0, c0), pl.ds(c1, c2 - c1))
+        high = (pl.ds(c0, c1 - c0), pl.ds(c2, end - c2))
+        self.parts = {"all": whole, "lo": low, "hi": high}
         self.send_sem, self.recv_sem = send_sem, recv_sem
 
     def at(self, colour, a, b):
@@ -82,28 +89,42 @@
             device_id_type=MESH,
         )
 
-    def send(self, number, colour, block, to):
-        self.copy(self.buf.at[block, self.rows[colour]], number, to).start()
-
-    def onward(self, *sources):
-        for b in (1, -1, 2):
+    def send(self, number, colour, block, to, part="all"):
+        self.copy(self.buf.at[block, self.parts[part][colour]], number, to).start()
+
+    def onward(self, number, *sources):
+        for b in (1, -1) if self.relay else (1, -1, 2):
             for a in sources:
                 for c in (0, 1):
-                    self.send(2, c, self.at(c, a, 0), self.at(c, 0, b))
+                    where = number if self.relay else 5
+                    self.send(where, c, self.at(c, a, 0), self.at(c, 0, b))
+
+    def opposite(self, *sources):
+        for way, part in ((1, "lo"), (-1, "hi")):
+            for a in sources:
+                for c in (0, 1):
+                    self.send(5, c, self.at(c, a, -way), self.at(c, 0, way), part)
 
     def start(self):
-        for number, ways in ((0, (1, -1)), (1, (2,))):
+        for number, ways in ((0, (1, -1)), (2, (2,))):
             for a in ways:
                 for c in (0, 1):
                     self.send(number, c, self.tp, self.at(c, a, 0))
-        self.onward(0)
+        self.onward(1, 0)
 
     def stage(self, number):
-        self.copy(self.buf.at[pl.ds(0, (2, 1, 12)[number])], number, self.at(0, 1, 0)).wait_recv()
+        blocks = (2, 2, 1, 4, 2, 4 if self.relay else 12)[number]
+        self.copy(self.buf.at[pl.ds(0, blocks)], number, self.at(0, 1, 0)).wait_recv()
         if number == 0:
-            self.onward(-1, 1)
+            self.onward(3, -1, 1)
         elif number == 1:
-            self.onward(2)
+            self.opposite(0)
+        elif number == 2:
+            self.onward(4, 2)
+        elif number == 3:
+            self.opposite(-1, 1)
+        elif number == 4:
+            self.opposite(2)
 
     def drain(self):
         self.copy(self.buf.at[pl.ds(0, 15)], 0, self.at(0, 1, 0)).wait_send()
@@ -222,10 +243,10 @@
     tail_docs = remote(docs.at[:, pl.ds(LANES, LANES)], halo_docs, t_send.at[5], t_recv.at[5], sp=sp_at(1))
     tail.start()
     tail_docs.start()
-    def gather(number, buf, cut):
-        return Gather(buf, cut, tp, g_send.at[pl.ds(number, 1)], g_recv.at[number])
-
-    g1 = gather(0, x_buf, TOK // 2)
+    def gather(number, buf, cuts, relay=False):
+        return Gather(buf, cuts, tp, g_send.at[pl.ds(number, 1)], g_recv.at[number], relay)
+
+    g1 = gather(0, x_buf, (64, 128, 192))
     g1.start()
     tail.wait_recv()
 
@@ -238,7 +259,9 @@
     hp, hq = iota((HALO, HALO), 0), iota((HALO, HALO), 1) - HALO
     halo_same = (halo_marks == marks_col[:HALO]) & (sp > 0)
     g1.stage(0)
-    g1.stage(1)
+    g1.stage(2)
+
+    g1.stage(5)
 
     def columns(d):
         return pl.ds(pl.multiple_of(tp_at(d) * LANES, LANES), LANES)
@@ -247,8 +270,6 @@
     def _(d):
         source = down_hbm.at[0, :, columns(d)]
         remote(source, down_w.at[tp], t_send.at[1], t_recv.at[1], tp=tp_at(d)).start()
-
-    g1.stage(2)
 
     for load in loads[4:]:
         load.wait()
@@ -305,17 +326,17 @@
     own_slots = dot(spread[pl.ds(0, near)], normed[tp]).astype(BF16)
     slots[pl.ds(0, near)] = own_slots
     over_sp(slots, arrived, 0, [-d for unit in CHUNKS[0] for d in UNITS[unit]])
-    rest = pl.ds(near, PACKED - near)
-    slots[rest] = dot(spread[rest], normed[tp]).astype(BF16)
-    for chunk in (1, 2):
-        over_sp(slots, arrived, chunk, [-d for d in UNITS[chunk + 1]])
-
     tokens = jnp.concatenate([normed[i] for i in range(TP)], axis=1)
     both = dot_nt(tokens, shared_w[...])
     gate_part, up_part = both[:, :SHARED], both[:, SHARED:]
     units = gate_part * jax.nn.sigmoid(gate_part) * up_part
     shared[tp] = jnp.concatenate([units[: TOK // 2], units[TOK // 2 :]], axis=1).astype(BF16)
-    gathers = {"g0": gather(1, shared, TOK // 4)}
+    rest = pl.ds(near, PACKED - near)
+    slots[rest] = dot(spread[rest], normed[tp]).astype(BF16)
+    for chunk in (1, 2):
+        over_sp(slots, arrived, chunk, [-d for d in UNITS[chunk + 1]])
+
+    gathers = {"g0": gather(1, shared, (32, 64, 96))}
     gathers["g0"].start()
     mine, mine_end = BACK * SLOT, (BACK + 1) * SLOT
     ins, mids = (in0, in1, in2), (mid0, mid1, mid2)
@@ -338,7 +359,7 @@
         count = len(CHUNKS[chunk])
         tight = squeeze[pl.ds(0, count * ROWS), pl.ds(0, count * WIDE)]
         ins[chunk][tp] = dot(tight, jnp.concatenate(parts, axis=0)).astype(BF16)
-        gathers["i" + str(chunk)] = gather(2 + chunk, ins[chunk], CUTS[chunk])
+        gathers["i" + str(chunk)] = gather(2 + chunk, ins[chunk], CUTS[chunk], relay=True)
         gathers["i" + str(chunk)].start()
 
     def run_expert(chunk):
@@ -377,9 +398,9 @@
 
         else:
             gathers[op[:2]].stage(int(op[2]))
-            if op[0] == "i" and op[2] == "2":
+            if op[0] == "i" and op[2] == "5":
                 run_expert(int(op[1]))
-            elif op[0] == "h" and op[2] == "2":
+            elif op[0] == "h" and op[2] == "5":
                 run_down(int(op[1]))
 
     all_of(sdown_w, 2).wait_recv()
@@ -464,7 +485,7 @@
         pltpu.VMEM((WIDE, ROWS), BF16),
         dma((16,)),
     ]
-    scratch += [dma((8,)), dma((8, 3)), dma((7,)), dma((7,)), dma((6,)), dma((6,))]
+    scratch += [dma((8,)), dma((8, 6)), dma((7,)), dma((7,)), dma((6,)), dma((6,))]
     return pl.pallas_call(
         layer,
         out_shape=jax.ShapeDtypeStruct((TOK, LANES), BF16),

time: 98.1 us -> 93.9 us (0.957)
  Pallas kernels: 96.5 us -> 92.3 us
    pallas_call x1, Pallas kernels: 96.5 us -> 92.3 us  [shards(): pl.pallas_call(layer, out_shape=jax.ShapeDtypeStruct((TOK, LANES), BF16),...]
where the time goes in v5:
time: 93.9 us; the launch traced here: 93.8 us
  Pallas kernels  92.3 us (98%)
  local copies, waits for them, and re-layouts  1.47 us (2%)
    pallas_call x1, Pallas kernels, shards(): pl.pallas_call(layer, out_shape=jax.ShapeDtypeStruct((TOK, LANES), BF16),...  92.3 us

profile of v5, /device:TPU:1, one launch (start us, length us, event | category | flops | bytes accessed | tf_op | source)
XLA Modules:
  0.0 93.8 jit_solution(18006141225210824410)
XLA Ops:
  0.0 92.3 %shard_map.154 = bf16[256,128]{1,0:T(8,128)(2,1)} custom-call(s32[1,256]{1,0:T(1,128)} %bitcast.17, s32[2,256]{1,0:T(2,128)} %bitcast.15, f32[2,256]{1,0:T(2,128)} %bitcast.16, f32[1,2048]{1,0:T(1,128)} %bitcast.12, f32[1,2048]{1,0:T(1,128)} %bitcast.13, f32[1,2048]{1,0:T(1,128)} %bitcast.14, f32[1,128]{1,0:T(1,128)} %bitcast.18, f32[1,128]{1,0:T(1,128)} %bitcast.19, ...), custom_call_target="tpu_custom_call" | custom-call | tf_op jit(solution)/shard_map/pallas_call | solution.py:489
  92.3 1.5 %copy.18 = bf16[256,128]{1,0:T(8,128)(2,1)} copy(bf16[256,128]{1,0:T(8,128)(2,1)} %shard_map.154) | data formatting | bytes 131072

commit v6 on v5

--- a/solution.py
+++ b/solution.py
@@ -36,15 +36,17 @@
 WIDE = 8 * SLOT
 CUTS = ((96, 176, 272), (48, 96, 144), (48, 80, 128))
 ORDER = (
-    "g00 g02 s0 z0",
-    "z1 i00 i01 i02",
-    "i10 i11 i12 z2",
-    "i03 i13 i04 i14",
-    "i20 i21 i22 i05",
-    "i23 i24 i15 i25",
-    "h10 h12 h20 h22",
-    "g05 h00 h15 h02",
-    "h25 h05",
+    "g00 g01 g02 s0",
+    "z0 g03 z1 i00",
+    "g04 i01 i02 i10",
+    "i11 i12 z2 i03",
+    "i04 i13 i14 i20",
+    "i22 i05 i15 i25",
+    "g05 h10 h11 h12",
+    "h20 h21 h22 h13",
+    "h14 h00 h23 h01",
+    "h02 h24 h15 h03",
+    "h25 h04 h05",
 )
 
 F32 = jnp.float32
@@ -336,7 +338,7 @@
     for chunk in (1, 2):
         over_sp(slots, arrived, chunk, [-d for d in UNITS[chunk + 1]])
 
-    gathers = {"g0": gather(1, shared, (32, 64, 96))}
+    gathers = {"g0": gather(1, shared, (32, 64, 96), relay=True)}
     gathers["g0"].start()
     mine, mine_end = BACK * SLOT, (BACK + 1) * SLOT
     ins, mids = (in0, in1, in2), (mid0, mid1, mid2)
@@ -359,7 +361,7 @@
         count = len(CHUNKS[chunk])
         tight = squeeze[pl.ds(0, count * ROWS), pl.ds(0, count * WIDE)]
         ins[chunk][tp] = dot(tight, jnp.concatenate(parts, axis=0)).astype(BF16)
-        gathers["i" + str(chunk)] = gather(2 + chunk, ins[chunk], CUTS[chunk], relay=True)
+        gathers["i" + str(chunk)] = gather(2 + chunk, ins[chunk], CUTS[chunk], relay=chunk < 2)
         gathers["i" + str(chunk)].start()
 
     def run_expert(chunk):
@@ -370,7 +372,7 @@
             gate_part = both[:, :LANES]
             value = gate_part * jax.nn.sigmoid(gate_part) * both[:, LANES:]
             mids[chunk][tp, rows] = value.astype(BF16)
-        gathers["h" + str(chunk)] = gather(5 + chunk, mids[chunk], CUTS[chunk])
+        gathers["h" + str(chunk)] = gather(5 + chunk, mids[chunk], CUTS[chunk], relay=True)
         gathers["h" + str(chunk)].start()
 
     def run_down(chunk):

time: 93.9 us -> 92.5 us (0.985)
  Pallas kernels: 92.3 us -> 90.9 us
    pallas_call x1, Pallas kernels: 92.3 us -> 90.9 us  [shards(): pl.pallas_call(layer, out_shape=jax.ShapeDtypeStruct((TOK, LANES), BF16),...]
where the time goes in v6:
time: 92.5 us; the launch traced here: 92.3 us
  Pallas kernels  90.9 us (98%)
  local copies, waits for them, and re-layouts  1.47 us (2%)
    pallas_call x1, Pallas kernels, shards(): pl.pallas_call(layer, out_shape=jax.ShapeDtypeStruct((TOK, LANES), BF16),...  90.9 us

profile of v6, /device:TPU:1, one launch (start us, length us, event | category | flops | bytes accessed | tf_op | source)
XLA Modules:
  0.0 92.3 jit_solution(17345844445222893319)
XLA Ops:
  0.0 90.9 %shard_map.154 = bf16[256,128]{1,0:T(8,128)(2,1)} custom-call(s32[1,256]{1,0:T(1,128)} %bitcast.17, s32[2,256]{1,0:T(2,128)} %bitcast.15, f32[2,256]{1,0:T(2,128)} %bitcast.16, f32[1,2048]{1,0:T(1,128)} %bitcast.12, f32[1,2048]{1,0:T(1,128)} %bitcast.13, f32[1,2048]{1,0:T(1,128)} %bitcast.14, f32[1,128]{1,0:T(1,128)} %bitcast.18, f32[1,128]{1,0:T(1,128)} %bitcast.19, ...), custom_call_target="tpu_custom_call" | custom-call | tf_op jit(solution)/shard_map/pallas_call | solution.py:491
  90.9 1.5 %copy.18 = bf16[256,128]{1,0:T(8,128)(2,1)} copy(bf16[256,128]{1,0:T(8,128)(2,1)} %shard_map.154) | data formatting | bytes 131072
